TPU v7x, 32 devices: a whole 2x2x4 slice. The times are simulated.
32 devices in a mesh: dp: 4 (over y, x), kv: 4 (over z), tp: 2 (over core).
Axes of the slice: x: 2, y: 2, z: 4, core: 2. Of those that a mesh axis runs over, the one named last changes fastest.
Arguments:
- tokens: bfloat16 [4, 1280, 2048], P('dp', 'kv'), may hold values from -72 to 72
- w_query: bfloat16 [2048, 512], P(None, 'tp'), may hold values from -0.125 to 0.125
- key_weight: bfloat16 [2048, 256], P(None, 'tp'), may hold values from -0.125 to 0.125
- value_weight: bfloat16 [2048, 256], P(None, 'tp'), may hold values from -2.09375 to 2.09375
- w_out: bfloat16 [512, 2048], P(None, 'tp'), may hold values from -0.25 to 0.25
- chosen: int32 [4, 40, 16], P('dp', 'kv'), may hold values from -1 to 39, as said below
Outputs:
- mixed: bfloat16 [4, 1280, 2048], P('dp', 'kv', 'tp')
- log_mass: float32 [4, 4, 1280], P('dp', 'tp', 'kv')
Inputs may be any that keep to these rules, and one draw needn't show every extreme that they name: `chosen`: entry 0 of row i of a sequence is i; the other entries are distinct blocks before i, or -1 for an empty slot. The 10 rows of one index of kv together name at most one block held by any other index of kv; this bound is reached.
All inputs are finite; a program needn't handle non-finite values.
Results may differ from a plain program's by a relative error of at most 0.006.
The roundings to bfloat16 on the way count: a program that leaves them out, or rounds other values in their place, can miss the bound.
Values may be sent and summed in bfloat16 or wider, within the bound.
No kernel may reach another device: no remote copies, remote signals or barrier semaphores. Data moves between devices by JAX's collectives and lax.ppermute only.
A program may use at most 64 MiB of HBM per device.

v0:
```python
import jax
import jax.numpy as jnp
from jax import lax
from jax.sharding import PartitionSpec as P

HEAD_WIDTH = 128


def body(tokens, w_query, key_weight, value_weight, w_out, chosen):
    local_tokens = tokens[0]
    local_chosen = chosen[0]
    row_count = local_tokens.shape[0]
    blocks_here, select_count = local_chosen.shape
    block_rows = row_count // blocks_here
    kv_heads = key_weight.shape[1] // HEAD_WIDTH
    query_heads = w_query.shape[1] // HEAD_WIDTH
    heads_per_group = query_heads // kv_heads
    width_kv = kv_heads * HEAD_WIDTH
    devices = lax.axis_size("kv")
    my_index = lax.axis_index("kv")
    queries = jnp.dot(local_tokens, w_query, preferred_element_type=jnp.float32).astype(
        jnp.bfloat16
    )
    projected_keys = jnp.dot(local_tokens, key_weight, preferred_element_type=jnp.float32).astype(
        jnp.bfloat16
    )
    projected_values = jnp.dot(
        local_tokens, value_weight, preferred_element_type=jnp.float32
    ).astype(jnp.bfloat16)
    paired = jnp.concatenate([projected_keys, projected_values], axis=1)
    gathered = lax.all_gather(paired, "kv", axis=0, tiled=True)
    block_table = gathered.reshape(devices * blocks_here, block_rows, 2 * width_kv)
    lookup = jnp.maximum(local_chosen, 0)
    picked = jnp.take(block_table, lookup, axis=0)
    selected_keys = picked[..., :width_kv].reshape(
        blocks_here, select_count * block_rows, kv_heads, HEAD_WIDTH
    )
    selected_values = picked[..., width_kv:].reshape(
        blocks_here, select_count * block_rows, kv_heads, HEAD_WIDTH
    )
    grouped_queries = queries.reshape(
        blocks_here, block_rows, kv_heads, heads_per_group, HEAD_WIDTH
    )
    scores = jnp.einsum(
        "btkgd,bskd->bkgts", grouped_queries, selected_keys, preferred_element_type=jnp.float32
    ) * HEAD_WIDTH ** (-0.5)
    bounded_index = jnp.maximum(local_chosen, 0)
    key_pos = (
        bounded_index[..., None] * block_rows + jnp.arange(block_rows, dtype=jnp.int32)
    ).reshape(blocks_here, select_count * block_rows)
    key_live = jnp.repeat(local_chosen >= 0, block_rows, axis=1)
    block_ids = my_index * blocks_here + jnp.arange(blocks_here, dtype=jnp.int32)
    query_pos = block_ids[:, None] * block_rows + jnp.arange(block_rows, dtype=jnp.int32)[None, :]
    allowed = key_live[:, None, :] & (key_pos[:, None, :] <= query_pos[:, :, None])
    scores = jnp.where(allowed[:, None, None], scores, -jnp.inf)
    row_max = jnp.max(scores, axis=-1)
    weights = jnp.exp(scores - row_max[..., None])
    row_sum = jnp.sum(weights, axis=-1)
    probs_low = weights.astype(jnp.bfloat16)
    summed = jnp.einsum(
        "bkgts,bskd->btkgd", probs_low, selected_values, preferred_element_type=jnp.float32
    )
    attended = (
        (summed / row_sum.transpose(0, 3, 1, 2)[..., None])
        .astype(jnp.bfloat16)
        .reshape(row_count, query_heads * HEAD_WIDTH)
    )
    log_mass = (row_max + jnp.log(row_sum)).transpose(1, 2, 0, 3).reshape(query_heads, row_count)
    mixed = jnp.dot(
        lax.all_gather(attended, "tp", axis=1, tiled=True),
        w_out,
        preferred_element_type=jnp.float32,
    ).astype(jnp.bfloat16)
    return (mixed[None], log_mass[None])


def solution(mesh):
    in_specs = (
        P("dp", "kv", None),
        P(None, "tp"),
        P(None, "tp"),
        P(None, "tp"),
        P(None, "tp"),
        P("dp", "kv", None),
    )
    out_specs = (P("dp", "kv", "tp"), P("dp", "tp", "kv"))
    return jax.shard_map(body, mesh=mesh, in_specs=in_specs, out_specs=out_specs, check_vma=False)
```

profile of v0, /device:TPU:0, one launch (start us, length us, event | category | flops | bytes accessed | tf_op | source)
XLA Modules:
  0.0 39.9 jit_solution(1609023411895982091)
XLA Ops:
  0.6 0.0 copy-start
  0.6 0.0 copy-start.3
  0.7 0.8 %broadcast_compare_fusion.1 = (pred[1,10,16]{2,0,1:T(4,128)(4,1)S(1)}, pred[1,10,16]{2,0,1:T(4,128)(4,1)S(1)}) fusion(s32[1,10,16]{2,0,1:T(1,128)} %param.11), kind=kLoop, calls=%fused_computation.39 | loop fusion | flops 480 | bytes 960 | tf_op jit(solution)/shard_map/ge | solution.py:51
  1.5 0.7 %broadcast_multiply_fusion = (s32[1,10,16]{2,0,1:T(1,128)S(1)}, s32[10,16]{1,0:T(8,128)S(1)}) fusion(s32[1,10,16]{2,0,1:T(1,128)} %param.11), kind=kLoop, calls=%fused_computation.37 | loop fusion | flops 320 | bytes 1920 | tf_op jit(solution)/shard_map/mul | solution.py:49
  2.2 0.1 reshape.141
  2.3 0.0 copy-done
  2.3 1.6 %fusion.14 = bf16[320,128]{1,0:T(8,128)(2,1)S(1)} fusion(bf16[2048,128]{1,0:T(8,128)(2,1)} %param.8, bf16[1,320,2048]{2,1,0:T(8,128)(2,1)S(1)} %copy-done), kind=kOutput, calls=%fused_computation.18 | convolution fusion | flops 167813120 | bytes 1916928 | tf_op jit(solution)/shard_map/dot_general | solution.py:24
  3.9 0.0 copy-done.3
  3.9 0.5 %fusion.17 = bf16[320,128]{1,0:T(8,128)(2,1)S(1)} fusion(bf16[2048,128]{1,0:T(8,128)(2,1)S(1)} %copy-done.3, bf16[1,320,2048]{2,1,0:T(8,128)(2,1)S(1)} %copy-done), kind=kOutput, calls=%fused_computation.19 | convolution fusion | flops 167813120 | bytes 1916928 | tf_op jit(solution)/shard_map/dot_general | solution.py:27
  4.4 19.7 %all_gather.6 = bf16[1280,256]{1,0:T(8,128)(2,1)S(1)} all-gather(bf16[320,256]{1,0:T(8,128)(2,1)S(1)} %pad_maximum_fusion), channel_id=1, replica_groups=mesh['dp'=4,'kv'=4,'tp'=2] {'kv'}, dimensions={0}, use_global_device_ids=true | all-gather | bytes 819200 | tf_op jit(solution)/shard_map/all_gather | solution.py:31
  24.2 2.5 %gather_fusion = bf16[160,32,256]{2,1,0:T(8,128)(2,1)} fusion(bf16[40,32,256]{2,1,0:T(8,128)(2,1)S(1)} %bitcast.78, s32[1024]{0:T(1024)S(1)} %pad_clamp_fusion), kind=kCustom, calls=%fused_computation | custom fusion | bytes 5243520 | tf_op jit(solution)/shard_map/jit(_take)/gather | solution.py:34
  26.7 2.1 %broadcast_select_fusion = bf16[10,16,32,256]{3,2,1,0:T(8,128)(2,1)S(1)} fusion(bf16[10,16,32,256]{3,2,1,0:T(8,128)(2,1)} %bitcast.79, pred[10,16]{1,0:T(8,128)(4,1)S(1)} %get-tuple-element.11), kind=kLoop, calls=%fused_computation.1 | loop fusion | flops 1310720 | bytes 5243040 | tf_op jit(solution)/shard_map/jit(_take)/select_n | solution.py:34
  28.7 1.8 %fusion.28 = (bf16[10,16,32,128]{3,2,1,0:T(8,128)(2,1)S(1)}, bf16[10,16,32,128]{3,2,1,0:T(8,128)(2,1)}) fusion(bf16[10,16,32,256]{3,2,1,0:T(8,128)(2,1)S(1)} %broadcast_select_fusion), kind=kLoop, calls=%fused_computation.43 | loop fusion | bytes 5242880 | tf_op jit(solution)/shard_map/slice | solution.py:35
  30.5 0.1 broadcast_in_dim.38
  30.6 0.1 and.20
  30.7 0.1 add.65
  30.8 0.1 add.66
  30.9 0.1 add.68
  31.0 0.1 iota_add_fusion
  31.1 0.2 compare_and_fusion
  31.3 1.7 %fusion.9 = bf16[320,256]{1,0:T(8,128)(2,1)S(1)} fusion(bf16[2048,256]{1,0:T(8,128)(2,1)} %param.7, bf16[1,320,2048]{2,1,0:T(8,128)(2,1)S(1)} %copy-done), kind=kOutput, calls=%fused_computation.15 | convolution fusion | flops 335626240 | bytes 2523136 | tf_op jit(solution)/shard_map/dot_general | solution.py:21
  33.0 0.7 %fusion.29 = (f32[10,2,32]{2,1,0:T(2,128)S(1)}, f32[10,1,2,32,512]{4,3,2,0,1:T(8,128)S(1)}) fusion(bf16[10,512,128,1]{2,1,3,0:T(8,128)(2,1)S(1)} %bitcast.80, bf16[10,32,2,128]{3,2,1,0:T(2,128)(2,1)S(1)} %reshape.136, pred[10,32,512]{2,1,0:T(8,128)(4,1)S(1)} %compare_and_fusion), kind=kOutput, calls=%fused_computation.44 | convolution fusion | flops 84868480 | bytes 2951680 | tf_op jit(solution)/shard_map/btkgd,bskd->bkgts/dot_general | solution.py:44
  33.7 0.0 copy-start.1
  33.7 0.5 %fusion.12 = f32[10,2,32]{2,1,0:T(2,128)S(1)} fusion(f32[10,1,2,32,512]{4,3,2,0,1:T(8,128)S(1)} %get-tuple-element.9, f32[10,2,32]{2,1,0:T(2,128)S(1)} %get-tuple-element.8), kind=kLoop, calls=%fused_computation.16 | loop fusion | flops 654720 | bytes 1315840 | tf_op jit(solution)/shard_map/reduce_sum | solution.py:58
  34.2 0.9 %copy-done.1 = bf16[10,16,32,128]{3,2,1,0:T(8,128)(2,1)S(1)} copy-done((bf16[10,16,32,128]{3,2,1,0:T(8,128)(2,1)S(1)}, bf16[10,16,32,128]{3,2,1,0:T(8,128)(2,1)}, u32[]{:S(2)}) %copy-start.1) | copy-done | bytes 1310744
  35.0 0.5 %fusion.21 = bf16[10,32,1,2,128]{4,1,3,0,2:T(8,128)(2,1)S(1)} fusion(bf16[10,512,128,1]{2,1,3,0:T(8,128)(2,1)S(1)} %bitcast.81, f32[10,1,2,32,512]{4,3,2,0,1:T(8,128)S(1)} %get-tuple-element.9, f32[10,2,32]{2,1,0:T(2,128)S(1)} %get-tuple-element.8, f32[10,32,2]{1,2,0:T(2,128)S(1)} %bitcast.84), kind=kOutput, calls=%fused_computation.21 | convolution fusion | flops 84705280 | bytes 2790400 | tf_op jit(solution)/shard_map/bkgts,bskd->btkgd/dot_general | solution.py:60
  35.5 0.0 copy-start.2
  35.5 0.1 copy.15
  35.7 2.2 %all_gather.7 = bf16[320,512]{1,0:T(8,128)(2,1)S(1)} all-gather(bf16[320,256]{1,0:T(8,128)(2,1)S(1)} %bitcast.83), channel_id=1, replica_groups=mesh['dp'=4,'kv'=4,'tp'=2] {'tp'}, dimensions={1}, use_global_device_ids=true | all-gather | bytes 491520 | tf_op jit(solution)/shard_map/all_gather | solution.py:70
  37.9 0.0 copy-done.2
  37.9 1.3 %fusion.8 = bf16[1,320,1024]{2,1,0:T(8,128)(2,1)} fusion(bf16[320,512]{1,0:T(8,128)(2,1)S(1)} %all_gather.7, bf16[512,1024]{1,0:T(8,128)(2,1)S(1)} %copy-done.2), kind=kOutput, calls=%fused_computation.13 | convolution fusion | flops 335872000 | bytes 2031616 | tf_op jit(solution)/shard_map/dot_general | solution.py:69
  39.2 0.7 %broadcast_in_dim_reshape.2 = f32[1,2,320]{2,1,0:T(2,128)} reshape(f32[1,2,10,32]{3,2,1,0:T(8,128)S(1)} %copy.16) | data formatting | bytes 5120 | tf_op jit(solution)/shard_map/broadcast_in_dim;reshape | solution.py:74
  (11 shorter events, 0.1 us)
Async XLA Ops:
  0.6 1.7 %copy-start = (bf16[1,320,2048]{2,1,0:T(8,128)(2,1)S(1)}, bf16[1,320,2048]{2,1,0:T(8,128)(2,1)}, u32[]{:S(2)}) copy-start(bf16[1,320,2048]{2,1,0:T(8,128)(2,1)} %param.6) | copy-start | bytes 3932164
  0.6 3.2 %copy-start.3 = (bf16[2048,128]{1,0:T(8,128)(2,1)S(1)}, bf16[2048,128]{1,0:T(8,128)(2,1)}, u32[]{:S(2)}) copy-start(bf16[2048,128]{1,0:T(8,128)(2,1)} %param.9) | copy-start | bytes 1572868
  33.7 1.3 %copy-start.1 = (bf16[10,16,32,128]{3,2,1,0:T(8,128)(2,1)S(1)}, bf16[10,16,32,128]{3,2,1,0:T(8,128)(2,1)}, u32[]{:S(2)}) copy-start(bf16[10,16,32,128]{3,2,1,0:T(8,128)(2,1)} %get-tuple-element.3) | copy-start | bytes 3932164
  35.5 2.4 %copy-start.2 = (bf16[512,1024]{1,0:T(8,128)(2,1)S(1)}, bf16[512,1024]{1,0:T(8,128)(2,1)}, u32[]{:S(2)}) copy-start(bf16[512,1024]{1,0:T(8,128)(2,1)} %param.10) | copy-start | bytes 3145732
where the time goes:
time: 40.2 us; the launch traced here: 39.9 us
  blocking collectives  21.9 us (54%)
  local copies, waits for them, and re-layouts  6.55 us (16%)
  matrix products  6.27 us (16%)
  other arithmetic  4.39 us (11%)
  between operations  0.81 us (2%)
    all_gather x1, blocking collectives, body(): gathered = lax.all_gather(paired, 'kv', axis=0, tiled=True)  19.7 us
    gather x1, local copies, waits for them, and re-layouts, body(): picked = jnp.take(block_table, lookup, axis=0)  2.49 us
    all_gather x1, blocking collectives, body(): lax.all_gather(attended, 'tp', axis=1, tiled=True)  2.17 us
    select_n x1, other arithmetic, body(): picked = jnp.take(block_table, lookup, axis=0)  2.05 us
    slice x1, local copies, waits for them, and re-layouts, body(): picked[..., :width_kv]  1.77 us
    dot_general x1, matrix products, body(): jnp.dot(local_tokens, w_query, preferred_element_type=jnp.float32)  1.73 us
    dot_general x1, matrix products, body(): jnp.dot(local_tokens, key_weight, preferred_element_type=jnp.float32)  1.55 us
    dot_general x1, matrix products, body(): jnp.dot(lax.all_gather(attended, 'tp', axis=1, tiled=True), w_out, prefer...  1.35 us

commit v1 on v0

v1 whole, which is shorter than its diff:
```python
import functools

import jax
import jax.numpy as jnp
from jax import lax
from jax.experimental import pallas as pl
from jax.experimental.pallas import tpu as pltpu
from jax.sharding import PartitionSpec as P

HEAD_WIDTH = 128
LOG2E = 1.4426950408889634
VMEM = pl.BlockSpec(memory_space=pltpu.VMEM)


def xor_distances(count):
    span = 1
    while span < count:
        span *= 2
    return list(range(1, span))


def exchange(value, distance, count):
    pairs = [(i, i ^ distance) for i in range(count) if (i ^ distance) < count]
    return lax.ppermute(value, "kv", pairs)


def pick_kernel(blocks_here, block_rows, far_count, *refs):
    kv_ref = refs[0]
    asked_refs = refs[1 : 1 + far_count]
    out_refs = refs[1 + far_count :]
    base = lax.axis_index("kv") * blocks_here
    rows = blocks_here * block_rows
    offset = lax.broadcasted_iota(jnp.int32, (block_rows, rows), 1) - lax.broadcasted_iota(
        jnp.int32, (block_rows, rows), 0
    )
    kv = kv_ref[...]
    for asked_ref, out_ref in zip(asked_refs, out_refs):
        asked = asked_ref[...]
        mine = (asked >= base) & (asked < base + blocks_here)
        local = jnp.max(jnp.where(mine, asked - base, -1), axis=(0, 1), keepdims=True)
        hot = jnp.where(offset == local * block_rows, 1.0, 0.0).astype(jnp.bfloat16)
        out_ref[...] = jnp.dot(hot, kv, preferred_element_type=jnp.float32).astype(jnp.bfloat16)


def attend_kernel(
    blocks_here, block_rows, distances, heads, chosen_ref, q_ref, kv_ref, *refs
):
    far_refs = refs[: len(distances)]
    out_ref, mass_ref = refs[len(distances) :]
    my_index = lax.axis_index("kv")
    rows = blocks_here * block_rows
    far_rows = len(distances) * block_rows
    keys = rows + far_rows
    chosen = chosen_ref[...]
    slots = chosen.shape[1]
    column = lax.broadcasted_iota(jnp.int32, (1, keys), 1)
    low = my_index * blocks_here + column // block_rows
    high = low + 1
    for at, distance in enumerate(distances):
        start = rows + at * block_rows
        here = (column >= start) & (column < start + block_rows)
        owner = jnp.bitwise_xor(my_index, distance)
        low = jnp.where(here, owner * blocks_here, low)
        high = jnp.where(here, (owner + 1) * blocks_here, high)
    member = jnp.zeros((blocks_here, keys), jnp.bool_)
    for slot in range(slots):
        entry = chosen[:, slot : slot + 1]
        member = member | ((entry >= low) & (entry < high))
    member = jnp.where(member, 1.0, 0.0).astype(jnp.bfloat16)
    spread = (
        lax.broadcasted_iota(jnp.int32, (blocks_here, rows), 1) // block_rows
        == lax.broadcasted_iota(jnp.int32, (blocks_here, rows), 0)
    )
    spread = jnp.where(spread, 1.0, 0.0).astype(jnp.bfloat16)
    named = lax.dot_general(
        member, spread, (((0,), (0,)), ((), ())), preferred_element_type=jnp.float32
    )
    key_at = lax.broadcasted_iota(jnp.int32, (keys, rows), 0)
    query_at = lax.broadcasted_iota(jnp.int32, (keys, rows), 1)
    allowed = (named > 0.5) & ((key_at <= query_at) | (key_at >= rows))
    key_rows = jnp.concatenate(
        [kv_ref[:, :HEAD_WIDTH]] + [far[:, :HEAD_WIDTH] for far in far_refs], axis=0
    )
    value_rows = jnp.concatenate(
        [kv_ref[:, HEAD_WIDTH:]] + [far[:, HEAD_WIDTH:] for far in far_refs], axis=0
    )
    scale = HEAD_WIDTH ** (-0.5)
    for head in range(heads):
        lanes = slice(head * HEAD_WIDTH, (head + 1) * HEAD_WIDTH)
        raw = lax.dot_general(
            key_rows, q_ref[:, lanes], (((1,), (1,)), ((), ())), preferred_element_type=jnp.float32
        )
        raw = jnp.where(allowed, raw, -jnp.inf)
        top = jnp.max(raw, axis=0, keepdims=True)
        weights = jnp.exp2((raw - top) * (scale * LOG2E))
        total = jnp.sum(weights, axis=0, keepdims=True)
        summed = lax.dot_general(
            value_rows,
            weights.astype(jnp.bfloat16),
            (((0,), (0,)), ((), ())),
            preferred_element_type=jnp.float32,
        )
        out_ref[:, lanes] = (summed / total).T.astype(jnp.bfloat16)
        mass_ref[head : head + 1, :] = top * scale + jnp.log(total)


def mix_kernel(own_ref, other_ref, w_ref, out_ref):
    width = own_ref.shape[1]
    side = lax.axis_index("tp")
    own_w = w_ref[pl.ds(pl.multiple_of(side * width, width), width), :]
    other_w = w_ref[pl.ds(pl.multiple_of((1 - side) * width, width), width), :]
    mixed = jnp.dot(own_ref[...], own_w, preferred_element_type=jnp.float32)
    mixed += jnp.dot(other_ref[...], other_w, preferred_element_type=jnp.float32)
    out_ref[...] = mixed.astype(jnp.bfloat16)


def body(tokens, w_query, key_weight, value_weight, w_out, chosen):
    local_tokens = tokens[0]
    local_chosen = chosen[0]
    rows = local_tokens.shape[0]
    blocks_here = local_chosen.shape[0]
    block_rows = rows // blocks_here
    heads = w_query.shape[1] // HEAD_WIDTH
    count = lax.axis_size("kv")
    distances = xor_distances(count)
    asked = [exchange(local_chosen, distance, count) for distance in distances]

    def project(weight):
        return jnp.dot(local_tokens, weight, preferred_element_type=jnp.float32).astype(
            jnp.bfloat16
        )

    paired = jnp.concatenate([project(key_weight), project(value_weight)], axis=1)
    queries = project(w_query)
    block = jax.ShapeDtypeStruct((block_rows, paired.shape[1]), jnp.bfloat16)
    picked = pl.pallas_call(
        functools.partial(pick_kernel, blocks_here, block_rows, len(distances)),
        out_shape=[block] * len(distances),
        in_specs=[VMEM] * (1 + len(distances)),
        out_specs=[VMEM] * len(distances),
        name="pick",
    )(paired, *asked)
    far = [exchange(rows_out, distance, count) for rows_out, distance in zip(picked, distances)]
    attended, log_mass = pl.pallas_call(
        functools.partial(attend_kernel, blocks_here, block_rows, distances, heads),
        out_shape=[
            jax.ShapeDtypeStruct((rows, heads * HEAD_WIDTH), jnp.bfloat16),
            jax.ShapeDtypeStruct((heads, rows), jnp.float32),
        ],
        in_specs=[VMEM] * (3 + len(distances)),
        out_specs=[VMEM] * 2,
        name="attend",
    )(local_chosen, queries, paired, *far)
    other = lax.ppermute(attended, "tp", [(0, 1), (1, 0)])
    mixed = pl.pallas_call(
        mix_kernel,
        out_shape=jax.ShapeDtypeStruct((rows, w_out.shape[1]), jnp.bfloat16),
        in_specs=[VMEM] * 3,
        out_specs=VMEM,
        name="mix",
    )(attended, other, w_out)
    return (mixed[None], log_mass[None])


def solution(mesh):
    in_specs = (
        P("dp", "kv", None),
        P(None, "tp"),
        P(None, "tp"),
        P(None, "tp"),
        P(None, "tp"),
        P("dp", "kv", None),
    )
    out_specs = (P("dp", "kv", "tp"), P("dp", "tp", "kv"))
    return jax.shard_map(body, mesh=mesh, in_specs=in_specs, out_specs=out_specs, check_vma=False)
```

time: 40.2 us -> 32 us (0.80)
  blocking collectives: 21.9 us -> 0 us
  starting transfers between devices: 0 us -> 10 us
  Pallas kernels: 0 us -> 7.66 us
  waiting for transfers between devices: 0 us -> 6.16 us
  other arithmetic: 4.39 us -> 0.67 us
  local copies, waits for them, and re-layouts: 6.55 us -> 3.29 us
  matrix products: 6.27 us -> 3.23 us
    all_gather x2 -> x0, blocking collectives: 21.9 us -> none  [the longest x1 19.7 us: body(): gathered = lax.all_gather(paired, 'kv', axis=0, tiled=True)]
    ppermute x0 -> x7, starting transfers between devices: none -> 10 us  [the longest x6 10 us: exchange(): return lax.ppermute(value, 'kv', pairs)]
    pallas_call x0 -> x3, Pallas kernels: none -> 7.66 us  [the longest x1 2.95 us: body(): pl.pallas_call(functools.partial(attend_kernel, blocks_here, block_rows,...]
    ppermute x0 -> x7, waiting for transfers between devices: none -> 6.16 us  [the longest x6 4.55 us: exchange(): return lax.ppermute(value, 'kv', pairs)]
    dot_general x6 -> x3, matrix products: 6.27 us -> 3.23 us  [project(): jnp.dot(local_tokens, weight, preferred_element_type=jnp.float32)]
    gather x1 -> x0, local copies, waits for them, and re-layouts: 2.49 us -> none  [body(): picked = jnp.take(block_table, lookup, axis=0)]
    unnamed x11 -> x23, local copies, waits for them, and re-layouts: 0.92 us -> 3.29 us
    select_n x1 -> x0, other arithmetic: 2.05 us -> none  [body(): picked = jnp.take(block_table, lookup, axis=0)]
  transfers between devices with their start and end apart: 0 -> 7, of which waited for: 0 -> 3; matrix products, arithmetic and copies ran while one was open for 0% -> 12% of each run, Pallas kernels for 0% -> 0%
where the time goes in v1:
time: 32 us; the launch traced here: 31.8 us
  starting transfers between devices  10 us (31%)
  Pallas kernels  7.66 us (24%)
  waiting for transfers between devices  6.16 us (19%)
  local copies, waits for them, and re-layouts  3.29 us (10%)
  matrix products  3.23 us (10%)
  between operations  0.72 us (2%)
  other arithmetic  0.67 us (2%)
    ppermute x6, starting transfers between devices, exchange(): return lax.ppermute(value, 'kv', pairs)  10 us
    ppermute x6, waiting for transfers between devices, exchange(): return lax.ppermute(value, 'kv', pairs)  4.55 us
    unnamed x23, local copies, waits for them, and re-layouts  3.29 us
    dot_general x3, matrix products, project(): jnp.dot(local_tokens, weight, preferred_element_type=jnp.float32)  3.23 us
    pallas_call x1, Pallas kernels, body(): pl.pallas_call(functools.partial(attend_kernel, blocks_here, block_rows,...  2.95 us
    pallas_call x1, Pallas kernels, body(): pl.pallas_call(mix_kernel, out_shape=jax.ShapeDtypeStruct((rows, w_out.sh...  2.74 us
    pallas_call x1, Pallas kernels, body(): pl.pallas_call(functools.partial(pick_kernel, blocks_here, block_rows, le...  1.97 us
    ppermute x1, waiting for transfers between devices, body(): other = lax.ppermute(attended, 'tp', [(0, 1), (1, 0)])  1.6 us
  transfers between devices with their start and end apart: 7, of which 3 were waited for; matrix products, arithmetic and copies ran while one was open for 12% of the time, Pallas kernels for 0%

profile of v1, /device:TPU:0, one launch (start us, length us, event | category | flops | bytes accessed | tf_op | source)
XLA Modules:
  0.0 31.8 jit_solution(14060398384262602639)
XLA Ops:
  0.6 0.0 copy-start
  0.6 0.0 copy-start.1
  0.7 0.8 %copy.10 = s32[1,10,16]{2,1,0:T(8,128)S(1)} copy(s32[1,10,16]{2,0,1:T(1,128)} %param.11) | data formatting | bytes 1280
  1.5 0.0 copy-start.3
  1.5 5.1 %collective-permute-start.2 = (s32[10,16]{1,0:T(8,128)S(1)}, s32[10,16]{1,0:T(8,128)S(1)}, u32[]{:S(2)}, u32[]{:S(2)}) collective-permute-start(s32[10,16]{1,0:T(8,128)S(1)} %bitcast.22), channel_id=1, source_target_pairs={{0,6},{2,4},{4,2},{6,0},{1,7},{3,5},{5,3},{7,1},{8,14},{10,12},{12... | collective-permute-start | bytes 1928 | tf_op jit(solution)/shard_map/ppermute | solution.py:24
  6.6 0.0 collective-permute-start.1
  6.6 0.6 %collective-permute-start = (s32[10,16]{1,0:T(8,128)S(1)}, s32[10,16]{1,0:T(8,128)S(1)}, u32[]{:S(2)}, u32[]{:S(2)}) collective-permute-start(s32[10,16]{1,0:T(8,128)S(1)} %bitcast.24), channel_id=1, source_target_pairs={{0,2},{2,0},{4,6},{6,4},{1,3},{3,1},{5,7},{7,5},{8,10},{10,8},{12,... | collective-permute-start | bytes 1928 | tf_op jit(solution)/shard_map/ppermute | solution.py:24
  7.1 0.0 copy-done
  7.1 1.5 %fusion.9 = bf16[320,128]{1,0:T(8,128)(2,1)S(1)} fusion(bf16[2048,128]{1,0:T(8,128)(2,1)} %param.8, bf16[1,320,2048]{2,1,0:T(8,128)(2,1)S(1)} %copy-done), kind=kOutput, calls=%fused_computation.7 | convolution fusion | flops 167813120 | bytes 1916928 | tf_op jit(solution)/shard_map/dot_general | solution.py:129
  8.7 0.0 copy-done.1
  8.7 0.0 copy-start.10
  8.7 0.5 %fusion.12 = bf16[320,128]{1,0:T(8,128)(2,1)S(1)} fusion(bf16[2048,128]{1,0:T(8,128)(2,1)S(1)} %copy-done.1, bf16[1,320,2048]{2,1,0:T(8,128)(2,1)S(1)} %copy-done), kind=kOutput, calls=%fused_computation.8 | convolution fusion | flops 167813120 | bytes 1916928 | tf_op jit(solution)/shard_map/dot_general | solution.py:129
  9.2 0.0 copy-done.3
  9.2 0.7 %pad_maximum_fusion.refs_0_.kv_ref = bf16[320,256]{1,0:T(8,128)(2,1)} fusion(bf16[320,128]{1,0:T(8,128)(2,1)S(1)} %fusion.12, bf16[320,128]{1,0:T(8,128)(2,1)S(1)} %fusion.9), kind=kLoop, calls=%fused_computation.9 | loop fusion | flops 327680 | bytes 327680 | tf_op jit(solution)/shard_map/concatenate | solution.py:133
  9.9 0.0 collective-permute-done.2.refs_3_
  9.9 0.0 copy-start.7
  9.9 1.2 %collective-permute-done.1.refs_2_ = s32[10,16]{1,0:T(8,128)S(1)} collective-permute-done((s32[10,16]{1,0:T(8,128)S(1)}, s32[10,16]{1,0:T(8,128)S(1)}, u32[]{:S(2)}, u32[]{:S(2)}) %collective-permute-start.1) | collective-permute-done | bytes 672 | tf_op jit(solution)/shard_map/ppermute | solution.py:24
  11.1 0.0 copy-start.8
  11.1 0.0 collective-permute-done.refs_1_
  11.1 0.0 copy-done.7
  11.1 0.6 %copy-done.8 = s32[10,16]{1,0:T(8,128)} copy-done((s32[10,16]{1,0:T(8,128)}, s32[10,16]{1,0:T(8,128)S(1)}, u32[]{:S(2)}) %copy-start.8) | copy-done | bytes 664
  11.7 0.0 copy-start.9
  11.7 0.6 %copy-done.9 = s32[10,16]{1,0:T(8,128)} copy-done((s32[10,16]{1,0:T(8,128)}, s32[10,16]{1,0:T(8,128)S(1)}, u32[]{:S(2)}) %copy-start.9) | copy-done | bytes 664
  12.3 2.0 %pick.1 = (bf16[32,256]{1,0:T(8,128)(2,1)}, bf16[32,256]{1,0:T(8,128)(2,1)}, bf16[32,256]{1,0:T(8,128)(2,1)}) custom-call(bf16[320,256]{1,0:T(8,128)(2,1)} %pad_maximum_fusion.refs_0_.kv_ref, s32[10,16]{1,0:T(8,128)} %copy-done.9, s32[10,16]{1,0:T(8,128)} %copy-done.8, s32[10,16]{1,0:T(8,128)} %copy-done.7), custom_call_target="tpu_custom_call" | custom-call | tf_op jit(solution)/shard_map/pick/pallas_call | solution.py:136
  14.3 0.3 collective-permute-start.3
  14.5 2.9 %collective-permute-start.4 = (bf16[32,256]{1,0:T(8,128)(2,1)}, bf16[32,256]{1,0:T(8,128)(2,1)S(1)}, u32[]{:S(2)}, u32[]{:S(2)}) collective-permute-start(bf16[32,256]{1,0:T(8,128)(2,1)} %get-tuple-element.8), channel_id=1, source_target_pairs={{0,4},{2,6},{4,0},{6,2},{1,5},{3,7},{5,1},{7,3},{8,12},{10,14},{12... | collective-permute-start | bytes 49160 | tf_op jit(solution)/shard_map/ppermute | solution.py:24
  17.5 1.2 %collective-permute-start.5 = (bf16[32,256]{1,0:T(8,128)(2,1)}, bf16[32,256]{1,0:T(8,128)(2,1)S(1)}, u32[]{:S(2)}, u32[]{:S(2)}) collective-permute-start(bf16[32,256]{1,0:T(8,128)(2,1)} %get-tuple-element.9), channel_id=1, source_target_pairs={{0,6},{2,4},{4,2},{6,0},{1,7},{3,5},{5,3},{7,1},{8,14},{10,12},{12... | collective-permute-start | bytes 49160 | tf_op jit(solution)/shard_map/ppermute | solution.py:24
  18.7 0.0 copy-done.10
  18.7 1.2 %fusion.6.q_ref = bf16[320,256]{1,0:T(8,128)(2,1)} fusion(bf16[2048,256]{1,0:T(8,128)(2,1)S(1)} %copy-done.10, bf16[1,320,2048]{2,1,0:T(8,128)(2,1)S(1)} %copy-done), kind=kOutput, calls=%fused_computation.6 | convolution fusion | flops 335626240 | bytes 2523136 | tf_op jit(solution)/shard_map/dot_general | solution.py:129
  19.8 0.0 collective-permute-done.3.refs_0_
  19.8 0.0 copy-start.4
  19.8 0.0 collective-permute-done.4.refs_1_
  19.8 0.0 copy-start.5
  19.9 3.3 %collective-permute-done.5.refs_2_ = bf16[32,256]{1,0:T(8,128)(2,1)S(1)} collective-permute-done((bf16[32,256]{1,0:T(8,128)(2,1)}, bf16[32,256]{1,0:T(8,128)(2,1)S(1)}, u32[]{:S(2)}, u32[]{:S(2)}) %collective-permute-start.5) | collective-permute-done | bytes 16416 | tf_op jit(solution)/shard_map/ppermute | solution.py:24
  23.2 0.0 copy-done.4
  23.2 0.0 copy-done.5
  23.2 0.0 copy-start.6
  23.2 0.6 %copy-done.6 = bf16[32,256]{1,0:T(8,128)(2,1)} copy-done((bf16[32,256]{1,0:T(8,128)(2,1)}, bf16[32,256]{1,0:T(8,128)(2,1)S(1)}, u32[]{:S(2)}) %copy-start.6) | copy-done | bytes 16408
  23.8 2.9 %attend.1 = (bf16[320,256]{1,0:T(8,128)(2,1)}, f32[2,320]{1,0:T(2,128)}) custom-call(s32[10,16]{1,0:T(8,128)} %bitcast.25, bf16[320,256]{1,0:T(8,128)(2,1)} %fusion.6.q_ref, bf16[320,256]{1,0:T(8,128)(2,1)} %pad_maximum_fusion.refs_0_.kv_ref, bf16[32,256]{1,0:T(8,128)(2,1)} %copy-done.4, bf16[32,256]{1,0:T(8,128)(2,1)} %copy-done.5, bf16[32,256]{1,0:T(8,128)(2,1)} %copy-done.6), custom_call_target="tpu_custom_call" | custom-call | tf_op jit(solution)/shard_map/attend/pallas_call | solution.py:144
  26.8 0.0 collective-permute-start.6
  26.8 1.6 %collective-permute-done.6.other_ref = bf16[320,256]{1,0:T(8,128)(2,1)S(1)} collective-permute-done((bf16[320,256]{1,0:T(8,128)(2,1)}, bf16[320,256]{1,0:T(8,128)(2,1)S(1)}, u32[]{:S(2)}, u32[]{:S(2)}) %collective-permute-start.6) | collective-permute-done | bytes 163872 | tf_op jit(solution)/shard_map/ppermute | solution.py:154
  28.4 0.0 copy-start.2
  28.4 0.7 %copy-done.2 = bf16[320,256]{1,0:T(8,128)(2,1)} copy-done((bf16[320,256]{1,0:T(8,128)(2,1)}, bf16[320,256]{1,0:T(8,128)(2,1)S(1)}, u32[]{:S(2)}) %copy-start.2) | copy-done | bytes 163864
  29.0 2.7 %mix.1 = bf16[320,1024]{1,0:T(8,128)(2,1)} custom-call(bf16[320,256]{1,0:T(8,128)(2,1)} %get-tuple-element.10.own_ref, bf16[320,256]{1,0:T(8,128)(2,1)} %copy-done.2, bf16[512,1024]{1,0:T(8,128)(2,1)} %w_ref.1), custom_call_target="tpu_custom_call" | custom-call | tf_op jit(solution)/shard_map/mix/pallas_call | solution.py:155
Async XLA Ops:
  0.6 6.5 %copy-start = (bf16[1,320,2048]{2,1,0:T(8,128)(2,1)S(1)}, bf16[1,320,2048]{2,1,0:T(8,128)(2,1)}, u32[]{:S(2)}) copy-start(bf16[1,320,2048]{2,1,0:T(8,128)(2,1)} %param.6) | copy-start | bytes 3932164
  0.6 8.0 %copy-start.1 = (bf16[2048,128]{1,0:T(8,128)(2,1)S(1)}, bf16[2048,128]{1,0:T(8,128)(2,1)}, u32[]{:S(2)}) copy-start(bf16[2048,128]{1,0:T(8,128)(2,1)} %param.9) | copy-start | bytes 1572868
  1.5 7.7 %copy-start.3 = (s32[1,10,16]{2,1,0:T(8,128)}, s32[1,10,16]{2,1,0:T(8,128)S(1)}, u32[]{:S(2)}) copy-start(s32[1,10,16]{2,1,0:T(8,128)S(1)} %copy.10) | copy-start | bytes 1924
  1.5 8.4 %collective-permute-start.2 = (s32[10,16]{1,0:T(8,128)S(1)}, s32[10,16]{1,0:T(8,128)S(1)}, u32[]{:S(2)}, u32[]{:S(2)}) collective-permute-start(s32[10,16]{1,0:T(8,128)S(1)} %bitcast.22), channel_id=1, source_target_pairs={{0,6},{2,4},{4,2},{6,0},{1,7},{3,5},{5,3},{7,1},{8,14},{10,12},{12... | collective-permute-start | bytes 1928 | tf_op jit(solution)/shard_map/ppermute | solution.py:24
  6.6 4.5 %collective-permute-start.1 = (s32[10,16]{1,0:T(8,128)S(1)}, s32[10,16]{1,0:T(8,128)S(1)}, u32[]{:S(2)}, u32[]{:S(2)}) collective-permute-start(s32[10,16]{1,0:T(8,128)S(1)} %bitcast.23), channel_id=1, source_target_pairs={{0,4},{2,6},{4,0},{6,2},{1,5},{3,7},{5,1},{7,3},{8,12},{10,14},{12... | collective-permute-start | bytes 1928 | tf_op jit(solution)/shard_map/ppermute | solution.py:24
  6.6 4.6 %collective-permute-start = (s32[10,16]{1,0:T(8,128)S(1)}, s32[10,16]{1,0:T(8,128)S(1)}, u32[]{:S(2)}, u32[]{:S(2)}) collective-permute-start(s32[10,16]{1,0:T(8,128)S(1)} %bitcast.24), channel_id=1, source_target_pairs={{0,2},{2,0},{4,6},{6,4},{1,3},{3,1},{5,7},{7,5},{8,10},{10,8},{12,... | collective-permute-start | bytes 1928 | tf_op jit(solution)/shard_map/ppermute | solution.py:24
  8.7 10.0 %copy-start.10 = (bf16[2048,256]{1,0:T(8,128)(2,1)S(1)}, bf16[2048,256]{1,0:T(8,128)(2,1)}, u32[]{:S(2)}) copy-start(bf16[2048,256]{1,0:T(8,128)(2,1)} %param.7) | copy-start | bytes 3145732
  9.9 1.2 %copy-start.7 = (s32[10,16]{1,0:T(8,128)}, s32[10,16]{1,0:T(8,128)S(1)}, u32[]{:S(2)}) copy-start(s32[10,16]{1,0:T(8,128)S(1)} %collective-permute-done.2.refs_3_) | copy-start | bytes 1924
  11.1 0.6 %copy-start.8 = (s32[10,16]{1,0:T(8,128)}, s32[10,16]{1,0:T(8,128)S(1)}, u32[]{:S(2)}) copy-start(s32[10,16]{1,0:T(8,128)S(1)} %collective-permute-done.1.refs_2_) | copy-start | bytes 1924
  11.7 0.6 %copy-start.9 = (s32[10,16]{1,0:T(8,128)}, s32[10,16]{1,0:T(8,128)S(1)}, u32[]{:S(2)}) copy-start(s32[10,16]{1,0:T(8,128)S(1)} %collective-permute-done.refs_1_) | copy-start | bytes 1924
  14.3 5.6 %collective-permute-start.3 = (bf16[32,256]{1,0:T(8,128)(2,1)}, bf16[32,256]{1,0:T(8,128)(2,1)S(1)}, u32[]{:S(2)}, u32[]{:S(2)}) collective-permute-start(bf16[32,256]{1,0:T(8,128)(2,1)} %get-tuple-element.7), channel_id=1, source_target_pairs={{0,2},{2,0},{4,6},{6,4},{1,3},{3,1},{5,7},{7,5},{8,10},{10,8},{12,... | collective-permute-start | bytes 49160 | tf_op jit(solution)/shard_map/ppermute | solution.py:24
  14.5 5.3 %collective-permute-start.4 = (bf16[32,256]{1,0:T(8,128)(2,1)}, bf16[32,256]{1,0:T(8,128)(2,1)S(1)}, u32[]{:S(2)}, u32[]{:S(2)}) collective-permute-start(bf16[32,256]{1,0:T(8,128)(2,1)} %get-tuple-element.8), channel_id=1, source_target_pairs={{0,4},{2,6},{4,0},{6,2},{1,5},{3,7},{5,1},{7,3},{8,12},{10,14},{12... | collective-permute-start | bytes 49160 | tf_op jit(solution)/shard_map/ppermute | solution.py:24
  17.5 5.7 %collective-permute-start.5 = (bf16[32,256]{1,0:T(8,128)(2,1)}, bf16[32,256]{1,0:T(8,128)(2,1)S(1)}, u32[]{:S(2)}, u32[]{:S(2)}) collective-permute-start(bf16[32,256]{1,0:T(8,128)(2,1)} %get-tuple-element.9), channel_id=1, source_target_pairs={{0,6},{2,4},{4,2},{6,0},{1,7},{3,5},{5,3},{7,1},{8,14},{10,12},{12... | collective-permute-start | bytes 49160 | tf_op jit(solution)/shard_map/ppermute | solution.py:24
  19.8 3.4 %copy-start.4 = (bf16[32,256]{1,0:T(8,128)(2,1)}, bf16[32,256]{1,0:T(8,128)(2,1)S(1)}, u32[]{:S(2)}) copy-start(bf16[32,256]{1,0:T(8,128)(2,1)S(1)} %collective-permute-done.3.refs_0_) | copy-start | bytes 49156
  19.8 3.4 %copy-start.5 = (bf16[32,256]{1,0:T(8,128)(2,1)}, bf16[32,256]{1,0:T(8,128)(2,1)S(1)}, u32[]{:S(2)}) copy-start(bf16[32,256]{1,0:T(8,128)(2,1)S(1)} %collective-permute-done.4.refs_1_) | copy-start | bytes 49156
  23.2 0.6 %copy-start.6 = (bf16[32,256]{1,0:T(8,128)(2,1)}, bf16[32,256]{1,0:T(8,128)(2,1)S(1)}, u32[]{:S(2)}) copy-start(bf16[32,256]{1,0:T(8,128)(2,1)S(1)} %collective-permute-done.5.refs_2_) | copy-start | bytes 49156
  26.8 1.6 %collective-permute-start.6 = (bf16[320,256]{1,0:T(8,128)(2,1)}, bf16[320,256]{1,0:T(8,128)(2,1)S(1)}, u32[]{:S(2)}, u32[]{:S(2)}) collective-permute-start(bf16[320,256]{1,0:T(8,128)(2,1)} %get-tuple-element.10.own_ref), channel_id=1, source_target_pairs={{0,1},{1,0},{2,3},{3,2},{4,5},{5,4},{6,7},{7,6},{8,9},{9,8},{10,11... | collective-permute-start | bytes 491528 | tf_op jit(solution)/shard_map/ppermute | solution.py:154
  28.4 0.7 %copy-start.2 = (bf16[320,256]{1,0:T(8,128)(2,1)}, bf16[320,256]{1,0:T(8,128)(2,1)S(1)}, u32[]{:S(2)}) copy-start(bf16[320,256]{1,0:T(8,128)(2,1)S(1)} %collective-permute-done.6.other_ref) | copy-start | bytes 491524

commit v2 on v1

v2 whole, which is shorter than its diff:
```python
import functools

import jax
import jax.numpy as jnp
from jax import lax
from jax.experimental import pallas as pl
from jax.experimental.pallas import tpu as pltpu
from jax.sharding import PartitionSpec as P

HEAD_WIDTH = 128
LOG2E = 1.4426950408889634
VMEM = pl.BlockSpec(memory_space=pltpu.VMEM)


def xor_distances(count):
    span = 1
    while span < count:
        span *= 2
    return list(range(1, span))


def exchange(value, distance, count):
    pairs = [(i, i ^ distance) for i in range(count) if (i ^ distance) < count]
    return lax.ppermute(value, "kv", pairs)


def grant(*sizes):
    return pltpu.CompilerParams(vmem_limit_bytes=(4 << 20) + 4 * sum(sizes))


def pick_kernel(blocks_here, block_rows, far_count, *refs):
    kv_ref = refs[0]
    asked_refs = refs[1 : 1 + far_count]
    out_refs = refs[1 + far_count :]
    base = lax.axis_index("kv") * blocks_here
    rows = blocks_here * block_rows
    offset = lax.broadcasted_iota(jnp.int32, (block_rows, rows), 1) - lax.broadcasted_iota(
        jnp.int32, (block_rows, rows), 0
    )
    kv = kv_ref[...]
    for asked_ref, out_ref in zip(asked_refs, out_refs):
        asked = asked_ref[:, 0, :]
        mine = (asked >= base) & (asked < base + blocks_here)
        local = jnp.max(jnp.where(mine, asked - base, -1), axis=(0, 1), keepdims=True)
        hot = jnp.where(offset == local * block_rows, 1.0, 0.0).astype(jnp.bfloat16)
        out_ref[...] = jnp.dot(hot, kv, preferred_element_type=jnp.float32).astype(jnp.bfloat16)


def named_pairs(chosen, low, high, spread):
    member = (chosen[:, :1] >= low) & (chosen[:, :1] < high)
    for slot in range(1, chosen.shape[1]):
        entry = chosen[:, slot : slot + 1]
        member = member | ((entry >= low) & (entry < high))
    member = jnp.where(member, 1.0, 0.0).astype(jnp.bfloat16)
    return (
        lax.dot_general(
            member, spread, (((0,), (0,)), ((), ())), preferred_element_type=jnp.float32
        )
        > 0.5
    )


def local_kernel(
    blocks_here, block_rows, distances, heads, chosen_ref, q_ref, kv_ref,
    sum_ref, stat_ref, bias_ref,
):
    my_index = lax.axis_index("kv")
    rows = blocks_here * block_rows
    chosen = chosen_ref[:, 0, :]
    spread = (
        lax.broadcasted_iota(jnp.int32, (blocks_here, rows), 1) // block_rows
        == lax.broadcasted_iota(jnp.int32, (blocks_here, rows), 0)
    )
    spread = jnp.where(spread, 1.0, 0.0).astype(jnp.bfloat16)
    block_id = (
        my_index * blocks_here + lax.broadcasted_iota(jnp.int32, (1, rows), 1) // block_rows
    )
    named = named_pairs(chosen, block_id, block_id + 1, spread)
    key_at = lax.broadcasted_iota(jnp.int32, (rows, rows), 0)
    query_at = lax.broadcasted_iota(jnp.int32, (rows, rows), 1)
    allowed = named & (key_at <= query_at)
    far_rows = len(distances) * block_rows
    column = lax.broadcasted_iota(jnp.int32, (1, far_rows), 1)
    low = jnp.zeros((1, far_rows), jnp.int32)
    for at, distance in enumerate(distances):
        here = (column >= at * block_rows) & (column < (at + 1) * block_rows)
        low = jnp.where(here, jnp.bitwise_xor(my_index, distance) * blocks_here, low)
    far_named = named_pairs(chosen, low, low + blocks_here, spread)
    bias_ref[...] = jnp.where(far_named, 0.0, -jnp.inf)
    scale = HEAD_WIDTH ** (-0.5) * LOG2E
    for head in range(heads):
        lanes = slice(head * HEAD_WIDTH, (head + 1) * HEAD_WIDTH)
        raw = lax.dot_general(
            kv_ref[:, :HEAD_WIDTH],
            q_ref[:, lanes],
            (((1,), (1,)), ((), ())),
            preferred_element_type=jnp.float32,
        )
        raw = jnp.where(allowed, raw, -jnp.inf)
        top = jnp.max(raw, axis=0, keepdims=True)
        weights = jnp.exp2((raw - top) * scale)
        sum_ref[lanes, :] = lax.dot_general(
            kv_ref[:, HEAD_WIDTH:],
            weights.astype(jnp.bfloat16),
            (((0,), (0,)), ((), ())),
            preferred_element_type=jnp.float32,
        )
        stat_ref[head : head + 1, :] = top
        stat_ref[heads + head : heads + head + 1, :] = jnp.sum(weights, axis=0, keepdims=True)


def far_kernel(heads, far_count, bias_ref, q_ref, sum_ref, stat_ref, *refs):
    far_refs = refs[:far_count]
    out_ref, mass_ref = refs[far_count:]
    key_rows = jnp.concatenate([far[:, :HEAD_WIDTH] for far in far_refs], axis=0)
    value_rows = jnp.concatenate([far[:, HEAD_WIDTH:] for far in far_refs], axis=0)
    scale = HEAD_WIDTH ** (-0.5)
    for head in range(heads):
        lanes = slice(head * HEAD_WIDTH, (head + 1) * HEAD_WIDTH)
        raw = lax.dot_general(
            key_rows, q_ref[:, lanes], (((1,), (1,)), ((), ())), preferred_element_type=jnp.float32
        )
        raw = raw + bias_ref[...]
        near_top = stat_ref[head : head + 1, :]
        top = jnp.maximum(near_top, jnp.max(raw, axis=0, keepdims=True))
        weights = jnp.exp2((raw - top) * (scale * LOG2E))
        keep = jnp.exp2((near_top - top) * (scale * LOG2E))
        total = stat_ref[heads + head : heads + head + 1, :] * keep + jnp.sum(
            weights, axis=0, keepdims=True
        )
        summed = sum_ref[lanes, :] * keep + lax.dot_general(
            value_rows,
            weights.astype(jnp.bfloat16),
            (((0,), (0,)), ((), ())),
            preferred_element_type=jnp.float32,
        )
        out_ref[:, lanes] = (summed / total).T.astype(jnp.bfloat16)
        mass_ref[head : head + 1, :] = top * scale + jnp.log(total)


def mix_kernel(step, own_ref, other_ref, w_ref, out_ref):
    width = own_ref.shape[1]
    side = lax.axis_index("tp")
    lanes = pl.ds(pl.multiple_of(pl.program_id(0) * step, step), step)
    own_w = w_ref[pl.ds(pl.multiple_of(side * width, width), width), lanes]
    other_w = w_ref[pl.ds(pl.multiple_of((1 - side) * width, width), width), lanes]
    mixed = jnp.dot(own_ref[...], own_w, preferred_element_type=jnp.float32)
    mixed += jnp.dot(other_ref[...], other_w, preferred_element_type=jnp.float32)
    out_ref[...] = mixed.astype(jnp.bfloat16)


def body(tokens, w_query, key_weight, value_weight, w_out, chosen):
    local_tokens = tokens[0]
    local_chosen = jnp.transpose(chosen, (1, 0, 2))
    rows = local_tokens.shape[0]
    blocks_here = local_chosen.shape[0]
    block_rows = rows // blocks_here
    heads = w_query.shape[1] // HEAD_WIDTH
    count = lax.axis_size("kv")
    distances = xor_distances(count)
    far_count = len(distances)
    far_rows = far_count * block_rows
    asked = [exchange(local_chosen, distance, count) for distance in distances]

    def project(weight):
        return jnp.dot(local_tokens, weight, preferred_element_type=jnp.float32).astype(
            jnp.bfloat16
        )

    paired = jnp.concatenate([project(key_weight), project(value_weight)], axis=1)
    queries = project(w_query)
    width = queries.shape[1]
    block = jax.ShapeDtypeStruct((block_rows, paired.shape[1]), jnp.bfloat16)
    picked = pl.pallas_call(
        functools.partial(pick_kernel, blocks_here, block_rows, far_count),
        out_shape=[block] * far_count,
        in_specs=[VMEM] * (1 + far_count),
        out_specs=[VMEM] * far_count,
        compiler_params=grant(rows * width),
        name="pick",
    )(paired, *asked)
    far = [exchange(rows_out, distance, count) for rows_out, distance in zip(picked, distances)]
    near_sum, near_stat, far_bias = pl.pallas_call(
        functools.partial(local_kernel, blocks_here, block_rows, distances, heads),
        out_shape=[
            jax.ShapeDtypeStruct((width, rows), jnp.float32),
            jax.ShapeDtypeStruct((2 * heads, rows), jnp.float32),
            jax.ShapeDtypeStruct((far_rows, rows), jnp.float32),
        ],
        in_specs=[VMEM] * 3,
        out_specs=[VMEM] * 3,
        compiler_params=grant(rows * width, rows * rows, far_rows * rows),
        name="near",
    )(local_chosen, queries, paired)
    attended, log_mass = pl.pallas_call(
        functools.partial(far_kernel, heads, far_count),
        out_shape=[
            jax.ShapeDtypeStruct((rows, width), jnp.bfloat16),
            jax.ShapeDtypeStruct((heads, rows), jnp.float32),
        ],
        in_specs=[VMEM] * (4 + far_count),
        out_specs=[VMEM] * 2,
        compiler_params=grant(rows * width, 3 * far_rows * rows),
        name="far",
    )(far_bias, queries, near_sum, near_stat, *far)
    other = lax.ppermute(attended, "tp", [(0, 1), (1, 0)])
    columns = w_out.shape[1]
    step = columns // 4
    mixed = pl.pallas_call(
        functools.partial(mix_kernel, step),
        out_shape=jax.ShapeDtypeStruct((rows, columns), jnp.bfloat16),
        grid=(4,),
        in_specs=[VMEM] * 3,
        out_specs=pl.BlockSpec((rows, step), lambda at: (0, at)),
        compiler_params=grant(rows * columns),
        name="mix",
    )(attended, other, w_out)
    return (mixed[None], log_mass[None])


def solution(mesh):
    in_specs = (
        P("dp", "kv", None),
        P(None, "tp"),
        P(None, "tp"),
        P(None, "tp"),
        P(None, "tp"),
        P("dp", "kv", None),
    )
    out_specs = (P("dp", "kv", "tp"), P("dp", "tp", "kv"))
    return jax.shard_map(body, mesh=mesh, in_specs=in_specs, out_specs=out_specs, check_vma=False)
```

time: 32 us -> 23.8 us (0.74)
  local copies, waits for them, and re-layouts: 3.29 us -> 0.03 us
  Pallas kernels: 7.66 us -> 5.12 us
  waiting for transfers between devices: 6.16 us -> 4.92 us
  other arithmetic: 0.67 us -> 0.02 us
  matrix products: 3.23 us -> 2.59 us
    unnamed x23 -> x10, local copies, waits for them, and re-layouts: 3.29 us -> 0.03 us
    pallas_call x3 -> x4, Pallas kernels: 7.66 us -> 5.12 us  [the longest x1 2.13 us: body(): pl.pallas_call(functools.partial(mix_kernel, step), out_shape=jax.ShapeDt...]
    ppermute x6, waiting for transfers between devices: 4.55 us -> 3.53 us  [exchange(): return lax.ppermute(value, 'kv', pairs)]
    concatenate x1, other arithmetic: 0.67 us -> 0.02 us  [body(): jnp.concatenate([project(key_weight), project(value_weight)], axis=1)]
    dot_general x3, matrix products: 3.23 us -> 2.59 us  [project(): jnp.dot(local_tokens, weight, preferred_element_type=jnp.float32)]
  transfers between devices with their start and end apart: 7 -> 7, of which waited for: 3 -> 3; matrix products, arithmetic and copies ran while one was open for 12% -> 11% of each run, Pallas kernels for 0% -> 6%
where the time goes in v2:
time: 23.8 us; the launch traced here: 23.6 us
  starting transfers between devices  10.2 us (43%)
  Pallas kernels  5.12 us (22%)
  waiting for transfers between devices  4.92 us (21%)
  matrix products  2.59 us (11%)
  between operations  0.76 us (3%)
    ppermute x6, starting transfers between devices, exchange(): return lax.ppermute(value, 'kv', pairs)  10.2 us
    ppermute x6, waiting for transfers between devices, exchange(): return lax.ppermute(value, 'kv', pairs)  3.53 us
    dot_general x3, matrix products, project(): jnp.dot(local_tokens, weight, preferred_element_type=jnp.float32)  2.59 us
    pallas_call x1, Pallas kernels, body(): pl.pallas_call(functools.partial(mix_kernel, step), out_shape=jax.ShapeDt...  2.13 us
    ppermute x1, waiting for transfers between devices, body(): other = lax.ppermute(attended, 'tp', [(0, 1), (1, 0)])  1.39 us
    pallas_call x1, Pallas kernels, body(): pl.pallas_call(functools.partial(local_kernel, blocks_here, block_rows, d...  1.37 us
    pallas_call x1, Pallas kernels, body(): pl.pallas_call(functools.partial(far_kernel, heads, far_count), out_shape...  1.19 us
  transfers between devices with their start and end apart: 7, of which 3 were waited for; matrix products, arithmetic and copies ran while one was open for 11% of the time, Pallas kernels for 6%

profile of v2, /device:TPU:0, one launch (start us, length us, event | category | flops | bytes accessed | tf_op | source)
XLA Modules:
  0.0 23.6 jit_solution(144618684518668163)
XLA Ops:
  0.6 0.0 copy-start
  0.6 0.0 copy-start.3
  0.7 5.1 %collective-permute-start.2 = (s32[10,1,16]{2,1,0:T(1,128)}, s32[10,1,16]{2,1,0:T(1,128)S(1)}, u32[]{:S(2)}, u32[]{:S(2)}) collective-permute-start(s32[10,1,16]{2,1,0:T(1,128)} %bitcast.19), channel_id=1, source_target_pairs={{0,6},{2,4},{4,2},{6,0},{1,7},{3,5},{5,3},{7,1},{8,14},{10,12},{12... | collective-permute-start | bytes 1928 | tf_op jit(solution)/shard_map/ppermute | solution.py:24
  5.8 0.0 collective-permute-start.1
  5.8 0.6 %collective-permute-start = (s32[10,1,16]{2,1,0:T(1,128)}, s32[10,1,16]{2,1,0:T(1,128)S(1)}, u32[]{:S(2)}, u32[]{:S(2)}) collective-permute-start(s32[10,1,16]{2,1,0:T(1,128)} %bitcast.21), channel_id=1, source_target_pairs={{0,2},{2,0},{4,6},{6,4},{1,3},{3,1},{5,7},{7,5},{8,10},{10,8},{12,... | collective-permute-start | bytes 1928 | tf_op jit(solution)/shard_map/ppermute | solution.py:24
  6.4 0.0 copy-done
  6.4 1.5 %fusion.9 = bf16[320,128]{1,0:T(8,128)(2,1)S(1)} fusion(bf16[2048,128]{1,0:T(8,128)(2,1)} %param.8, bf16[1,320,2048]{2,1,0:T(8,128)(2,1)S(1)} %copy-done), kind=kOutput, calls=%fused_computation.7 | convolution fusion | flops 167813120 | bytes 1916928 | tf_op jit(solution)/shard_map/dot_general | solution.py:166
  8.0 0.0 copy-done.3
  8.0 0.0 copy-start.4
  8.0 0.5 %fusion.12 = bf16[320,128]{1,0:T(8,128)(2,1)S(1)} fusion(bf16[2048,128]{1,0:T(8,128)(2,1)S(1)} %copy-done.3, bf16[1,320,2048]{2,1,0:T(8,128)(2,1)S(1)} %copy-done), kind=kOutput, calls=%fused_computation.8 | convolution fusion | flops 167813120 | bytes 1916928 | tf_op jit(solution)/shard_map/dot_general | solution.py:166
  8.6 0.0 collective-permute-done.2.refs_3_
  8.6 1.9 %collective-permute-done.1.refs_2_ = s32[10,1,16]{2,1,0:T(1,128)S(1)} collective-permute-done((s32[10,1,16]{2,1,0:T(1,128)}, s32[10,1,16]{2,1,0:T(1,128)S(1)}, u32[]{:S(2)}, u32[]{:S(2)}) %collective-permute-start.1) | collective-permute-done | bytes 672 | tf_op jit(solution)/shard_map/ppermute | solution.py:24
  10.5 0.0 collective-permute-done.refs_1_
  10.5 0.4 %pick.1 = (bf16[32,256]{1,0:T(8,128)(2,1)S(1)}, bf16[32,256]{1,0:T(8,128)(2,1)S(1)}, bf16[32,256]{1,0:T(8,128)(2,1)S(1)}) custom-call(bf16[320,256]{1,0:T(8,128)(2,1)S(1)} %pad_maximum_fusion.kv_ref.refs_0_, s32[10,1,16]{2,1,0:T(1,128)S(1)} %collective-permute-done.refs_1_, s32[10,1,16]{2,1,0:T(1,128)S(1)} %collective-permute-done.1.refs_2_, ...), custom_call_target="tpu_custom_call" | custom-call | tf_op jit(solution)/shard_map/pick/pallas_call | solution.py:174
  11.0 0.0 collective-permute-start.3
  11.0 2.4 %collective-permute-start.4 = (bf16[32,256]{1,0:T(8,128)(2,1)S(1)}, bf16[32,256]{1,0:T(8,128)(2,1)S(1)}, u32[]{:S(2)}, u32[]{:S(2)}) collective-permute-start(bf16[32,256]{1,0:T(8,128)(2,1)S(1)} %get-tuple-element.14), channel_id=1, source_target_pairs={{0,4},{2,6},{4,0},{6,2},{1,5},{3,7},{5,1},{7,3},{8,12},{10,14},{12... | collective-permute-start | bytes 49160 | tf_op jit(solution)/shard_map/ppermute | solution.py:24
  13.4 0.0 copy-start.2
  13.4 2.0 %collective-permute-start.5 = (bf16[32,256]{1,0:T(8,128)(2,1)S(1)}, bf16[32,256]{1,0:T(8,128)(2,1)S(1)}, u32[]{:S(2)}, u32[]{:S(2)}) collective-permute-start(bf16[32,256]{1,0:T(8,128)(2,1)S(1)} %get-tuple-element.15), channel_id=1, source_target_pairs={{0,6},{2,4},{4,2},{6,0},{1,7},{3,5},{5,3},{7,1},{8,14},{10,12},{12... | collective-permute-start | bytes 49160 | tf_op jit(solution)/shard_map/ppermute | solution.py:24
  15.4 0.0 copy-done.4
  15.4 0.5 %fusion.6.q_ref = bf16[320,256]{1,0:T(8,128)(2,1)S(1)} fusion(bf16[2048,256]{1,0:T(8,128)(2,1)S(1)} %copy-done.4, bf16[1,320,2048]{2,1,0:T(8,128)(2,1)S(1)} %copy-done), kind=kOutput, calls=%fused_computation.6 | convolution fusion | flops 335626240 | bytes 2523136 | tf_op jit(solution)/shard_map/dot_general | solution.py:166
  15.9 0.0 copy-done.2
  15.9 0.0 copy-start.1
  15.9 1.4 %near.1 = (f32[256,320]{1,0:T(8,128)S(1)}, f32[4,320]{1,0:T(4,128)S(1)}, f32[96,320]{1,0:T(8,128)S(1)}) custom-call(s32[10,1,16]{2,1,0:T(1,128)S(1)} %bitcast.22, bf16[320,256]{1,0:T(8,128)(2,1)S(1)} %fusion.6.q_ref, bf16[320,256]{1,0:T(8,128)(2,1)S(1)} %pad_maximum_fusion.kv_ref.refs_0_), custom_call_target="tpu_custom_call" | custom-call | tf_op jit(solution)/shard_map/near/pallas_call | solution.py:183
  17.3 0.0 collective-permute-done.3.refs_0_
  17.3 0.0 collective-permute-done.4.refs_1_
  17.3 1.6 %collective-permute-done.5.refs_2_ = bf16[32,256]{1,0:T(8,128)(2,1)S(1)} collective-permute-done((bf16[32,256]{1,0:T(8,128)(2,1)S(1)}, bf16[32,256]{1,0:T(8,128)(2,1)S(1)}, u32[]{:S(2)}, u32[]{:S(2)}) %collective-permute-start.5) | collective-permute-done | bytes 16416 | tf_op jit(solution)/shard_map/ppermute | solution.py:24
  18.9 1.2 %far.1 = (bf16[320,256]{1,0:T(8,128)(2,1)S(1)}, f32[2,320]{1,0:T(2,128)}) custom-call(f32[96,320]{1,0:T(8,128)S(1)} %get-tuple-element.10.bias_ref, bf16[320,256]{1,0:T(8,128)(2,1)S(1)} %fusion.6.q_ref, f32[256,320]{1,0:T(8,128)S(1)} %get-tuple-element.11.sum_ref, f32[4,320]{1,0:T(4,128)S(1)} %get-tuple-element.12.stat_ref, ...), custom_call_target="tpu_custom_call" | custom-call | tf_op jit(solution)/shard_map/far/pallas_call | solution.py:195
  20.1 0.0 collective-permute-start.6
  20.1 1.4 %collective-permute-done.6.other_ref = bf16[320,256]{1,0:T(8,128)(2,1)S(1)} collective-permute-done((bf16[320,256]{1,0:T(8,128)(2,1)S(1)}, bf16[320,256]{1,0:T(8,128)(2,1)S(1)}, u32[]{:S(2)}, u32[]{:S(2)}) %collective-permute-start.6) | collective-permute-done | bytes 163872 | tf_op jit(solution)/shard_map/ppermute | solution.py:206
  21.5 0.0 copy-done.1
  21.5 2.1 %mix.1 = bf16[320,1024]{1,0:T(8,128)(2,1)} custom-call(bf16[320,256]{1,0:T(8,128)(2,1)S(1)} %get-tuple-element.16.own_ref, bf16[320,256]{1,0:T(8,128)(2,1)S(1)} %collective-permute-done.6.other_ref, bf16[512,1024]{1,0:T(8,128)(2,1)S(1)} %copy-done.1), custom_call_target="tpu_custom_call" | custom-call | tf_op jit(solution)/shard_map/mix/pallas_call | solution.py:209
  (1 shorter events, 0.0 us)
Async XLA Ops:
  0.6 5.8 %copy-start = (bf16[1,320,2048]{2,1,0:T(8,128)(2,1)S(1)}, bf16[1,320,2048]{2,1,0:T(8,128)(2,1)}, u32[]{:S(2)}) copy-start(bf16[1,320,2048]{2,1,0:T(8,128)(2,1)} %param.6) | copy-start | bytes 3932164
  0.6 7.4 %copy-start.3 = (bf16[2048,128]{1,0:T(8,128)(2,1)S(1)}, bf16[2048,128]{1,0:T(8,128)(2,1)}, u32[]{:S(2)}) copy-start(bf16[2048,128]{1,0:T(8,128)(2,1)} %param.9) | copy-start | bytes 1572868
  0.7 7.9 %collective-permute-start.2 = (s32[10,1,16]{2,1,0:T(1,128)}, s32[10,1,16]{2,1,0:T(1,128)S(1)}, u32[]{:S(2)}, u32[]{:S(2)}) collective-permute-start(s32[10,1,16]{2,1,0:T(1,128)} %bitcast.19), channel_id=1, source_target_pairs={{0,6},{2,4},{4,2},{6,0},{1,7},{3,5},{5,3},{7,1},{8,14},{10,12},{12... | collective-permute-start | bytes 1928 | tf_op jit(solution)/shard_map/ppermute | solution.py:24
  5.8 4.7 %collective-permute-start.1 = (s32[10,1,16]{2,1,0:T(1,128)}, s32[10,1,16]{2,1,0:T(1,128)S(1)}, u32[]{:S(2)}, u32[]{:S(2)}) collective-permute-start(s32[10,1,16]{2,1,0:T(1,128)} %bitcast.20), channel_id=1, source_target_pairs={{0,4},{2,6},{4,0},{6,2},{1,5},{3,7},{5,1},{7,3},{8,12},{10,14},{12... | collective-permute-start | bytes 1928 | tf_op jit(solution)/shard_map/ppermute | solution.py:24
  5.8 4.7 %collective-permute-start = (s32[10,1,16]{2,1,0:T(1,128)}, s32[10,1,16]{2,1,0:T(1,128)S(1)}, u32[]{:S(2)}, u32[]{:S(2)}) collective-permute-start(s32[10,1,16]{2,1,0:T(1,128)} %bitcast.21), channel_id=1, source_target_pairs={{0,2},{2,0},{4,6},{6,4},{1,3},{3,1},{5,7},{7,5},{8,10},{10,8},{12,... | collective-permute-start | bytes 1928 | tf_op jit(solution)/shard_map/ppermute | solution.py:24
  8.0 7.4 %copy-start.4 = (bf16[2048,256]{1,0:T(8,128)(2,1)S(1)}, bf16[2048,256]{1,0:T(8,128)(2,1)}, u32[]{:S(2)}) copy-start(bf16[2048,256]{1,0:T(8,128)(2,1)} %param.7) | copy-start | bytes 3145732
  11.0 6.4 %collective-permute-start.3 = (bf16[32,256]{1,0:T(8,128)(2,1)S(1)}, bf16[32,256]{1,0:T(8,128)(2,1)S(1)}, u32[]{:S(2)}, u32[]{:S(2)}) collective-permute-start(bf16[32,256]{1,0:T(8,128)(2,1)S(1)} %get-tuple-element.13), channel_id=1, source_target_pairs={{0,2},{2,0},{4,6},{6,4},{1,3},{3,1},{5,7},{7,5},{8,10},{10,8},{12,... | collective-permute-start | bytes 49160 | tf_op jit(solution)/shard_map/ppermute | solution.py:24
  11.0 6.3 %collective-permute-start.4 = (bf16[32,256]{1,0:T(8,128)(2,1)S(1)}, bf16[32,256]{1,0:T(8,128)(2,1)S(1)}, u32[]{:S(2)}, u32[]{:S(2)}) collective-permute-start(bf16[32,256]{1,0:T(8,128)(2,1)S(1)} %get-tuple-element.14), channel_id=1, source_target_pairs={{0,4},{2,6},{4,0},{6,2},{1,5},{3,7},{5,1},{7,3},{8,12},{10,14},{12... | collective-permute-start | bytes 49160 | tf_op jit(solution)/shard_map/ppermute | solution.py:24
  13.4 2.5 %copy-start.2 = (s32[1,10,16]{2,0,1:T(1,128)S(1)}, s32[1,10,16]{2,0,1:T(1,128)}, u32[]{:S(2)}) copy-start(s32[1,10,16]{2,0,1:T(1,128)} %param.11) | copy-start | bytes 1924
  13.4 5.5 %collective-permute-start.5 = (bf16[32,256]{1,0:T(8,128)(2,1)S(1)}, bf16[32,256]{1,0:T(8,128)(2,1)S(1)}, u32[]{:S(2)}, u32[]{:S(2)}) collective-permute-start(bf16[32,256]{1,0:T(8,128)(2,1)S(1)} %get-tuple-element.15), channel_id=1, source_target_pairs={{0,6},{2,4},{4,2},{6,0},{1,7},{3,5},{5,3},{7,1},{8,14},{10,12},{12... | collective-permute-start | bytes 49160 | tf_op jit(solution)/shard_map/ppermute | solution.py:24
  15.9 5.6 %copy-start.1 = (bf16[512,1024]{1,0:T(8,128)(2,1)S(1)}, bf16[512,1024]{1,0:T(8,128)(2,1)}, u32[]{:S(2)}) copy-start(bf16[512,1024]{1,0:T(8,128)(2,1)} %w_ref.1) | copy-start | bytes 3145732
  20.1 1.4 %collective-permute-start.6 = (bf16[320,256]{1,0:T(8,128)(2,1)S(1)}, bf16[320,256]{1,0:T(8,128)(2,1)S(1)}, u32[]{:S(2)}, u32[]{:S(2)}) collective-permute-start(bf16[320,256]{1,0:T(8,128)(2,1)S(1)} %get-tuple-element.16.own_ref), channel_id=1, source_target_pairs={{0,1},{1,0},{2,3},{3,2},{4,5},{5,4},{6,7},{7,6},{8,9},{9,8},{10,11... | collective-permute-start | bytes 491528 | tf_op jit(solution)/shard_map/ppermute | solution.py:206

commit v3 on v2

--- a/solution.py
+++ b/solution.py
@@ -7,6 +7,7 @@
 from jax.experimental.pallas import tpu as pltpu
 from jax.sharding import PartitionSpec as P
 
+
 HEAD_WIDTH = 128
 LOG2E = 1.4426950408889634
 VMEM = pl.BlockSpec(memory_space=pltpu.VMEM)
@@ -24,26 +25,74 @@
     return lax.ppermute(value, "kv", pairs)
 
 
+def shared_exchange(value, distances, count):
+    pairs = [
+        (2 * i + t, 2 * (i ^ distance) + t)
+        for i in range(count)
+        for t, distance in enumerate(distances)
+        if (i ^ distance) < count
+    ]
+    return lax.ppermute(value, ("kv", "tp"), pairs)
+
+
+def swap(value):
+    return lax.ppermute(value, "tp", [(0, 1), (1, 0)])
+
+
 def grant(*sizes):
     return pltpu.CompilerParams(vmem_limit_bytes=(4 << 20) + 4 * sum(sizes))
 
 
-def pick_kernel(blocks_here, block_rows, far_count, *refs):
-    kv_ref = refs[0]
-    asked_refs = refs[1 : 1 + far_count]
-    out_refs = refs[1 + far_count :]
+def project_kernel(
+    chunks, tokens_ref, key_ref, value_ref, out_ref, tokens, weights, arrived
+):
+    width = key_ref.shape[1]
+    step = key_ref.shape[0] // chunks
+    copies = []
+    for at in range(chunks):
+        span = pl.ds(at * step, step)
+        moves = (
+            (tokens_ref.at[:, span], tokens.at[:, span]),
+            (key_ref.at[span], weights.at[span, pl.ds(0, width)]),
+            (value_ref.at[span], weights.at[span, pl.ds(width, width)]),
+        )
+        group = [
+            pltpu.make_async_copy(source, target, arrived.at[at, lane])
+            for lane, (source, target) in enumerate(moves)
+        ]
+        for copy in group:
+            copy.start()
+        copies.append(group)
+    total = None
+    for at in range(chunks):
+        for copy in copies[at]:
+            copy.wait()
+        span = slice(at * step, (at + 1) * step)
+        part = jnp.dot(tokens[:, span], weights[span, :], preferred_element_type=jnp.float32)
+        total = part if total is None else total + part
+    out_ref[...] = total.astype(jnp.bfloat16)
+
+
+def pick_kernel(blocks_here, block_rows, shared_count, alone_count, kv_ref, kv_other_ref, *refs):
+    asked_refs = refs[: shared_count + alone_count]
+    out_refs = refs[shared_count + alone_count :]
     base = lax.axis_index("kv") * blocks_here
     rows = blocks_here * block_rows
     offset = lax.broadcasted_iota(jnp.int32, (block_rows, rows), 1) - lax.broadcasted_iota(
         jnp.int32, (block_rows, rows), 0
     )
-    kv = kv_ref[...]
-    for asked_ref, out_ref in zip(asked_refs, out_refs):
+    for at, (asked_ref, out_ref) in enumerate(zip(asked_refs, out_refs)):
         asked = asked_ref[:, 0, :]
         mine = (asked >= base) & (asked < base + blocks_here)
         local = jnp.max(jnp.where(mine, asked - base, -1), axis=(0, 1), keepdims=True)
         hot = jnp.where(offset == local * block_rows, 1.0, 0.0).astype(jnp.bfloat16)
-        out_ref[...] = jnp.dot(hot, kv, preferred_element_type=jnp.float32).astype(jnp.bfloat16)
+        out_ref[:block_rows, :] = jnp.dot(
+            hot, kv_ref[...], preferred_element_type=jnp.float32
+        ).astype(jnp.bfloat16)
+        if at < shared_count:
+            out_ref[block_rows:, :] = jnp.dot(
+                hot, kv_other_ref[...], preferred_element_type=jnp.float32
+            ).astype(jnp.bfloat16)
 
 
 def named_pairs(chosen, low, high, spread):
@@ -61,7 +110,7 @@
 
 
 def local_kernel(
-    blocks_here, block_rows, distances, heads, chosen_ref, q_ref, kv_ref,
+    blocks_here, block_rows, far_order, heads, chosen_ref, q_ref, kv_ref,
     sum_ref, stat_ref, bias_ref,
 ):
     my_index = lax.axis_index("kv")
@@ -79,11 +128,13 @@
     key_at = lax.broadcasted_iota(jnp.int32, (rows, rows), 0)
     query_at = lax.broadcasted_iota(jnp.int32, (rows, rows), 1)
     allowed = named & (key_at <= query_at)
-    far_rows = len(distances) * block_rows
+    far_rows = len(far_order) * block_rows
     column = lax.broadcasted_iota(jnp.int32, (1, far_rows), 1)
     low = jnp.zeros((1, far_rows), jnp.int32)
-    for at, distance in enumerate(distances):
+    side = lax.axis_index("tp")
+    for at, by_side in enumerate(far_order):
         here = (column >= at * block_rows) & (column < (at + 1) * block_rows)
+        distance = jnp.where(side == 0, by_side[0], by_side[1])
         low = jnp.where(here, jnp.bitwise_xor(my_index, distance) * blocks_here, low)
     far_named = named_pairs(chosen, low, low + blocks_here, spread)
     bias_ref[...] = jnp.where(far_named, 0.0, -jnp.inf)
@@ -109,9 +160,12 @@
         stat_ref[heads + head : heads + head + 1, :] = jnp.sum(weights, axis=0, keepdims=True)
 
 
-def far_kernel(heads, far_count, bias_ref, q_ref, sum_ref, stat_ref, *refs):
-    far_refs = refs[:far_count]
-    out_ref, mass_ref = refs[far_count:]
+def far_kernel(
+    heads, block_rows, shared_count, alone_count, bias_ref, q_ref, sum_ref, stat_ref, *refs
+):
+    out_ref, mass_ref = refs[-2:]
+    far_refs = [ref.at[:block_rows] for ref in refs[: shared_count + alone_count]]
+    far_refs += list(refs[shared_count + alone_count : -2])
     key_rows = jnp.concatenate([far[:, :HEAD_WIDTH] for far in far_refs], axis=0)
     value_rows = jnp.concatenate([far[:, HEAD_WIDTH:] for far in far_refs], axis=0)
     scale = HEAD_WIDTH ** (-0.5)
@@ -138,14 +192,21 @@
         mass_ref[head : head + 1, :] = top * scale + jnp.log(total)
 
 
-def mix_kernel(step, own_ref, other_ref, w_ref, out_ref):
+def half_mix_kernel(own_ref, w_ref, out_ref):
     width = own_ref.shape[1]
-    side = lax.axis_index("tp")
+    start = lax.axis_index("tp") * width
+    own_w = w_ref[pl.ds(pl.multiple_of(start, width), width), :]
+    out_ref[...] = jnp.dot(own_ref[...], own_w, preferred_element_type=jnp.float32)
+
+
+def mix_kernel(step, half_ref, other_ref, w_ref, out_ref):
+    width = other_ref.shape[1]
+    start = (1 - lax.axis_index("tp")) * width
     lanes = pl.ds(pl.multiple_of(pl.program_id(0) * step, step), step)
-    own_w = w_ref[pl.ds(pl.multiple_of(side * width, width), width), lanes]
-    other_w = w_ref[pl.ds(pl.multiple_of((1 - side) * width, width), width), lanes]
-    mixed = jnp.dot(own_ref[...], own_w, preferred_element_type=jnp.float32)
-    mixed += jnp.dot(other_ref[...], other_w, preferred_element_type=jnp.float32)
+    other_w = w_ref[pl.ds(pl.multiple_of(start, width), width), lanes]
+    mixed = half_ref[:, lanes] + jnp.dot(
+        other_ref[...], other_w, preferred_element_type=jnp.float32
+    )
     out_ref[...] = mixed.astype(jnp.bfloat16)
 
 
@@ -158,30 +219,56 @@
     heads = w_query.shape[1] // HEAD_WIDTH
     count = lax.axis_size("kv")
     distances = xor_distances(count)
-    far_count = len(distances)
-    far_rows = far_count * block_rows
-    asked = [exchange(local_chosen, distance, count) for distance in distances]
-
-    def project(weight):
-        return jnp.dot(local_tokens, weight, preferred_element_type=jnp.float32).astype(
-            jnp.bfloat16
-        )
-
-    paired = jnp.concatenate([project(key_weight), project(value_weight)], axis=1)
-    queries = project(w_query)
-    width = queries.shape[1]
-    block = jax.ShapeDtypeStruct((block_rows, paired.shape[1]), jnp.bfloat16)
+    shared = list(zip(distances[0:-1:2], distances[1::2]))
+    alone = distances[2 * len(shared) :]
+    shared_count, alone_count = len(shared), len(alone)
+    far_order = shared + [(d, d) for d in alone] + [(b, a) for a, b in shared]
+    far_rows = len(far_order) * block_rows
+    asked = [shared_exchange(local_chosen, pair, count) for pair in shared]
+    asked += [exchange(local_chosen, distance, count) for distance in alone]
+    width = w_query.shape[1]
+    pair_width = key_weight.shape[1] + value_weight.shape[1]
+    depth = key_weight.shape[0]
+    chunks = 4
+    paired = pl.pallas_call(
+        functools.partial(project_kernel, chunks),
+        out_shape=jax.ShapeDtypeStruct((rows, pair_width), jnp.bfloat16),
+        in_specs=[pl.BlockSpec(memory_space=pltpu.HBM)] * 3,
+        out_specs=VMEM,
+        scratch_shapes=[
+            pltpu.VMEM((rows, depth), jnp.bfloat16),
+            pltpu.VMEM((depth, pair_width), jnp.bfloat16),
+            pltpu.SemaphoreType.DMA((chunks, 3)),
+        ],
+        compiler_params=grant(depth * pair_width, rows * depth),
+        name="project",
+    )(
+        *[
+            pltpu.with_memory_space_constraint(value, pltpu.HBM)
+            for value in (local_tokens, key_weight, value_weight)
+        ]
+    )
+    paired_other = swap(paired)
+    queries = jnp.dot(local_tokens, w_query, preferred_element_type=jnp.float32).astype(
+        jnp.bfloat16
+    )
+    two = jax.ShapeDtypeStruct((2 * block_rows, pair_width), jnp.bfloat16)
+    one = jax.ShapeDtypeStruct((block_rows, pair_width), jnp.bfloat16)
     picked = pl.pallas_call(
-        functools.partial(pick_kernel, blocks_here, block_rows, far_count),
-        out_shape=[block] * far_count,
-        in_specs=[VMEM] * (1 + far_count),
-        out_specs=[VMEM] * far_count,
-        compiler_params=grant(rows * width),
+        functools.partial(pick_kernel, blocks_here, block_rows, shared_count, alone_count),
+        out_shape=[two] * shared_count + [one] * alone_count,
+        in_specs=[VMEM] * (2 + shared_count + alone_count),
+        out_specs=[VMEM] * (shared_count + alone_count),
+        compiler_params=grant(rows * pair_width),
         name="pick",
-    )(paired, *asked)
-    far = [exchange(rows_out, distance, count) for rows_out, distance in zip(picked, distances)]
+    )(paired, paired_other, *asked)
+    far = [shared_exchange(value, pair, count) for value, pair in zip(picked, shared)]
+    far += [exchange(value, d, count) for value, d in zip(picked[shared_count:], alone)]
+    if shared:
+        crossing = [value[block_rows:] for value in far[:shared_count]]
+        far.append(swap(jnp.concatenate(crossing, axis=0) if shared_count > 1 else crossing[0]))
     near_sum, near_stat, far_bias = pl.pallas_call(
-        functools.partial(local_kernel, blocks_here, block_rows, distances, heads),
+        functools.partial(local_kernel, blocks_here, block_rows, far_order, heads),
         out_shape=[
             jax.ShapeDtypeStruct((width, rows), jnp.float32),
             jax.ShapeDtypeStruct((2 * heads, rows), jnp.float32),
@@ -193,18 +280,26 @@
         name="near",
     )(local_chosen, queries, paired)
     attended, log_mass = pl.pallas_call(
-        functools.partial(far_kernel, heads, far_count),
+        functools.partial(far_kernel, heads, block_rows, shared_count, alone_count),
         out_shape=[
             jax.ShapeDtypeStruct((rows, width), jnp.bfloat16),
             jax.ShapeDtypeStruct((heads, rows), jnp.float32),
         ],
-        in_specs=[VMEM] * (4 + far_count),
+        in_specs=[VMEM] * (4 + len(far)),
         out_specs=[VMEM] * 2,
         compiler_params=grant(rows * width, 3 * far_rows * rows),
         name="far",
     )(far_bias, queries, near_sum, near_stat, *far)
-    other = lax.ppermute(attended, "tp", [(0, 1), (1, 0)])
+    other = swap(attended)
     columns = w_out.shape[1]
+    half = pl.pallas_call(
+        half_mix_kernel,
+        out_shape=jax.ShapeDtypeStruct((rows, columns), jnp.float32),
+        in_specs=[VMEM] * 2,
+        out_specs=VMEM,
+        compiler_params=grant(rows * columns),
+        name="half",
+    )(attended, w_out)
     step = columns // 4
     mixed = pl.pallas_call(
         functools.partial(mix_kernel, step),
@@ -214,7 +309,7 @@
         out_specs=pl.BlockSpec((rows, step), lambda at: (0, at)),
         compiler_params=grant(rows * columns),
         name="mix",
-    )(attended, other, w_out)
+    )(half, other, w_out)
     return (mixed[None], log_mass[None])
 
 

time: 23.8 us -> 23.4 us (0.983)
  Pallas kernels: 5.12 us -> 7.82 us
  starting transfers between devices: 10.2 us -> 7.68 us
  matrix products: 2.59 us -> 0.53 us
  waiting for transfers between devices: 4.92 us -> 6.51 us
    ppermute x6 -> x2, starting transfers between devices: 10.2 us -> 6.5 us  [exchange(): return lax.ppermute(value, 'kv', pairs)]
    ppermute x1 -> x5, waiting for transfers between devices: 1.39 us -> 4.92 us  [the longest x2 4.23 us: shared_exchange(): return lax.ppermute(value, ('kv', 'tp'), pairs)]
    pallas_call x3 -> x5, Pallas kernels: 2.98 us -> 5.84 us  [the longest x1 2.55 us: body(): pl.pallas_call(functools.partial(project_kernel, chunks), out_shape=jax.S...]
    dot_general x3 -> x1, matrix products: 2.59 us -> 0.53 us  [body(): jnp.dot(local_tokens, w_query, preferred_element_type=jnp.float32)]
    ppermute x6 -> x2, waiting for transfers between devices: 3.53 us -> 1.6 us  [exchange(): return lax.ppermute(value, 'kv', pairs)]
    ppermute x1 -> x5, starting transfers between devices: 0.01 us -> 1.18 us  [the longest x3 1.06 us: swap(): return lax.ppermute(value, 'tp', [(0, 1), (1, 0)])]
  transfers between devices with their start and end apart: 7 -> 7, of which waited for: 3 -> 4; matrix products, arithmetic and copies ran while one was open for 11% -> 2% of each run, Pallas kernels for 6% -> 7%
where the time goes in v3:
time: 23.4 us; the launch traced here: 23.3 us
  Pallas kernels  7.82 us (33%)
  starting transfers between devices  7.68 us (33%)
  waiting for transfers between devices  6.51 us (28%)
  between operations  0.73 us (3%)
  matrix products  0.53 us (2%)
    ppermute x2, starting transfers between devices, exchange(): return lax.ppermute(value, 'kv', pairs)  6.5 us
    ppermute x2, waiting for transfers between devices, shared_exchange(): return lax.ppermute(value, ('kv', 'tp'), pairs)  4.23 us
    pallas_call x1, Pallas kernels, body(): pl.pallas_call(functools.partial(project_kernel, chunks), out_shape=jax.S...  2.55 us
    pallas_call x1, Pallas kernels, body(): pl.pallas_call(functools.partial(mix_kernel, step), out_shape=jax.ShapeDt...  1.98 us
    ppermute x2, waiting for transfers between devices, exchange(): return lax.ppermute(value, 'kv', pairs)  1.6 us
    pallas_call x1, Pallas kernels, body(): pl.pallas_call(functools.partial(local_kernel, blocks_here, block_rows, f...  1.37 us
    pallas_call x1, Pallas kernels, body(): pl.pallas_call(functools.partial(far_kernel, heads, block_rows, shared_co...  1.19 us
    ppermute x3, starting transfers between devices, swap(): return lax.ppermute(value, 'tp', [(0, 1), (1, 0)])  1.06 us
  transfers between devices with their start and end apart: 7, of which 4 were waited for; matrix products, arithmetic and copies ran while one was open for 2% of the time, Pallas kernels for 7%

profile of v3, /device:TPU:0, one launch (start us, length us, event | category | flops | bytes accessed | tf_op | source)
XLA Modules:
  0.0 23.3 jit_solution(15652598402265638459)
XLA Ops:
  0.6 0.0 copy-start
  0.6 0.0 copy-start.2
  0.7 0.0 copy-start.3
  0.7 2.5 %project.1.kv_ref = bf16[320,256]{1,0:T(8,128)(2,1)S(1)} custom-call(bf16[320,2048]{1,0:T(8,128)(2,1)} %bitcast.10, bf16[2048,128]{1,0:T(8,128)(2,1)} %key_ref.1, bf16[2048,128]{1,0:T(8,128)(2,1)} %value_ref.1), custom_call_target="tpu_custom_call" | custom-call | tf_op jit(solution)/shard_map/project/pallas_call | solution.py:233
  3.2 0.6 %collective-permute-start = (bf16[320,256]{1,0:T(8,128)(2,1)S(1)}, bf16[320,256]{1,0:T(8,128)(2,1)S(1)}, u32[]{:S(2)}, u32[]{:S(2)}) collective-permute-start(bf16[320,256]{1,0:T(8,128)(2,1)S(1)} %project.1.kv_ref), channel_id=1, source_target_pairs={{0,1},{1,0},{2,3},{3,2},{4,5},{5,4},{6,7},{7,6},{8,9},{9,8},{10,11... | collective-permute-start | bytes 491528 | tf_op jit(solution)/shard_map/ppermute | solution.py:39
  3.8 0.0 copy-done.2
  3.8 4.7 %collective-permute-start.2 = (s32[10,1,16]{2,1,0:T(1,128)S(1)}, s32[10,1,16]{2,1,0:T(1,128)S(1)}, u32[]{:S(2)}, u32[]{:S(2)}) collective-permute-start(s32[10,1,16]{2,1,0:T(1,128)S(1)} %bitcast.7), channel_id=1, source_target_pairs={{0,6},{2,4},{4,2},{6,0},{1,7},{3,5},{5,3},{7,1},{8,14},{10,12},{12... | collective-permute-start | bytes 1928 | tf_op jit(solution)/shard_map/ppermute | solution.py:25
  8.5 0.0 collective-permute-start.1
  8.5 1.6 %collective-permute-done.2.refs_1_ = s32[10,1,16]{2,1,0:T(1,128)S(1)} collective-permute-done((s32[10,1,16]{2,1,0:T(1,128)S(1)}, s32[10,1,16]{2,1,0:T(1,128)S(1)}, u32[]{:S(2)}, u32[]{:S(2)}) %collective-permute-start.2) | collective-permute-done | bytes 672 | tf_op jit(solution)/shard_map/ppermute | solution.py:25
  10.0 2.0 %collective-permute-done.1.refs_0_ = s32[10,1,16]{2,1,0:T(1,128)S(1)} collective-permute-done((s32[10,1,16]{2,1,0:T(1,128)S(1)}, s32[10,1,16]{2,1,0:T(1,128)S(1)}, u32[]{:S(2)}, u32[]{:S(2)}) %collective-permute-start.1) | collective-permute-done | bytes 672 | tf_op jit(solution)/shard_map/ppermute | solution.py:35
  12.1 0.0 collective-permute-done.kv_other_ref
  12.1 0.4 %pick.1 = (bf16[64,256]{1,0:T(8,128)(2,1)S(1)}, bf16[32,256]{1,0:T(8,128)(2,1)S(1)}) custom-call(bf16[320,256]{1,0:T(8,128)(2,1)S(1)} %project.1.kv_ref, bf16[320,256]{1,0:T(8,128)(2,1)S(1)} %collective-permute-done.kv_other_ref, s32[10,1,16]{2,1,0:T(1,128)S(1)} %collective-permute-done.1.refs_0_, s32[10,1,16]{2,1,0:T(1,128)S(1)} %collective-permute-done.2.refs_1_), custom_call_target="tpu_custom_call" | custom-call | tf_op jit(solution)/shard_map/pick/pallas_call | solution.py:257
  12.5 0.1 collective-permute-start.3
  12.6 1.8 %collective-permute-start.4 = (bf16[32,256]{1,0:T(8,128)(2,1)S(1)}, bf16[32,256]{1,0:T(8,128)(2,1)S(1)}, u32[]{:S(2)}, u32[]{:S(2)}) collective-permute-start(bf16[32,256]{1,0:T(8,128)(2,1)S(1)} %get-tuple-element.13), channel_id=1, source_target_pairs={{0,6},{2,4},{4,2},{6,0},{1,7},{3,5},{5,3},{7,1},{8,14},{10,12},{12... | collective-permute-start | bytes 49160 | tf_op jit(solution)/shard_map/ppermute | solution.py:25
  14.4 2.2 %collective-permute-done.3.refs_0_ = bf16[64,256]{1,0:T(8,128)(2,1)S(1)} collective-permute-done((bf16[64,256]{1,0:T(8,128)(2,1)S(1)}, bf16[64,256]{1,0:T(8,128)(2,1)S(1)}, u32[]{:S(2)}, u32[]{:S(2)}) %collective-permute-start.3) | collective-permute-done | bytes 32800 | tf_op jit(solution)/shard_map/ppermute | solution.py:35
  16.6 0.0 collective-permute-start.5
  16.6 0.0 copy-done
  16.6 0.0 copy-done.3
  16.7 0.5 %convolution_convert_fusion.q_ref = bf16[320,256]{1,0:T(8,128)(2,1)S(1)} fusion(bf16[2048,256]{1,0:T(8,128)(2,1)S(1)} %copy-done, bf16[1,320,2048]{2,1,0:T(8,128)(2,1)S(1)} %copy-done.3), kind=kOutput, calls=%fused_computation | convolution fusion | flops 335626240 | bytes 2523136 | tf_op jit(solution)/shard_map/dot_general | solution.py:252
  17.2 0.0 copy-start.1
  17.2 1.4 %near.1 = (f32[256,320]{1,0:T(8,128)S(1)}, f32[4,320]{1,0:T(4,128)S(1)}, f32[96,320]{1,0:T(8,128)S(1)}) custom-call(s32[10,1,16]{2,1,0:T(1,128)S(1)} %bitcast.9, bf16[320,256]{1,0:T(8,128)(2,1)S(1)} %convolution_convert_fusion.q_ref, bf16[320,256]{1,0:T(8,128)(2,1)S(1)} %project.1.kv_ref), custom_call_target="tpu_custom_call" | custom-call | tf_op jit(solution)/shard_map/near/pallas_call | solution.py:270
  18.6 0.0 collective-permute-done.4.refs_1_
  18.6 0.0 collective-permute-done.5.refs_2_
  18.6 1.2 %far.1 = (bf16[320,256]{1,0:T(8,128)(2,1)S(1)}, f32[2,320]{1,0:T(2,128)}) custom-call(f32[96,320]{1,0:T(8,128)S(1)} %get-tuple-element.9.bias_ref, bf16[320,256]{1,0:T(8,128)(2,1)S(1)} %convolution_convert_fusion.q_ref, f32[256,320]{1,0:T(8,128)S(1)} %get-tuple-element.10.sum_ref, f32[4,320]{1,0:T(4,128)S(1)} %get-tuple-element.11.stat_ref, ...), custom_call_target="tpu_custom_call" | custom-call | tf_op jit(solution)/shard_map/far/pallas_call | solution.py:282
  19.8 0.5 %collective-permute-start.6 = (bf16[320,256]{1,0:T(8,128)(2,1)S(1)}, bf16[320,256]{1,0:T(8,128)(2,1)S(1)}, u32[]{:S(2)}, u32[]{:S(2)}) collective-permute-start(bf16[320,256]{1,0:T(8,128)(2,1)S(1)} %get-tuple-element.14.own_ref), channel_id=1, source_target_pairs={{0,1},{1,0},{2,3},{3,2},{4,5},{5,4},{6,7},{7,6},{8,9},{9,8},{10,11... | collective-permute-start | bytes 491528 | tf_op jit(solution)/shard_map/ppermute | solution.py:39
  20.3 0.0 copy-done.1
  20.3 0.3 %half.1.half_ref = f32[320,1024]{1,0:T(8,128)S(1)} custom-call(bf16[320,256]{1,0:T(8,128)(2,1)S(1)} %get-tuple-element.14.own_ref, bf16[512,1024]{1,0:T(8,128)(2,1)S(1)} %copy-done.1), custom_call_target="tpu_custom_call" | custom-call | tf_op jit(solution)/shard_map/half/pallas_call | solution.py:295
  20.6 0.7 %collective-permute-done.6.other_ref = bf16[320,256]{1,0:T(8,128)(2,1)S(1)} collective-permute-done((bf16[320,256]{1,0:T(8,128)(2,1)S(1)}, bf16[320,256]{1,0:T(8,128)(2,1)S(1)}, u32[]{:S(2)}, u32[]{:S(2)}) %collective-permute-start.6) | collective-permute-done | bytes 163872 | tf_op jit(solution)/shard_map/ppermute | solution.py:39
  21.3 2.0 %mix.1 = bf16[320,1024]{1,0:T(8,128)(2,1)} custom-call(f32[320,1024]{1,0:T(8,128)S(1)} %half.1.half_ref, bf16[320,256]{1,0:T(8,128)(2,1)S(1)} %collective-permute-done.6.other_ref, bf16[512,1024]{1,0:T(8,128)(2,1)S(1)} %copy-done.1), custom_call_target="tpu_custom_call" | custom-call | tf_op jit(solution)/shard_map/mix/pallas_call | solution.py:304
  (1 shorter events, 0.0 us)
Async XLA Ops:
  0.6 16.0 %copy-start = (bf16[2048,256]{1,0:T(8,128)(2,1)S(1)}, bf16[2048,256]{1,0:T(8,128)(2,1)}, u32[]{:S(2)}) copy-start(bf16[2048,256]{1,0:T(8,128)(2,1)} %param.7) | copy-start | bytes 3145732
  0.6 3.1 %copy-start.2 = (s32[1,10,16]{2,0,1:T(1,128)S(1)}, s32[1,10,16]{2,0,1:T(1,128)}, u32[]{:S(2)}) copy-start(s32[1,10,16]{2,0,1:T(1,128)} %param.11) | copy-start | bytes 1924
  0.7 16.0 %copy-start.3 = (bf16[1,320,2048]{2,1,0:T(8,128)(2,1)S(1)}, bf16[1,320,2048]{2,1,0:T(8,128)(2,1)}, u32[]{:S(2)}) copy-start(bf16[1,320,2048]{2,1,0:T(8,128)(2,1)} %param.6) | copy-start | bytes 3932164
  3.2 8.9 %collective-permute-start = (bf16[320,256]{1,0:T(8,128)(2,1)S(1)}, bf16[320,256]{1,0:T(8,128)(2,1)S(1)}, u32[]{:S(2)}, u32[]{:S(2)}) collective-permute-start(bf16[320,256]{1,0:T(8,128)(2,1)S(1)} %project.1.kv_ref), channel_id=1, source_target_pairs={{0,1},{1,0},{2,3},{3,2},{4,5},{5,4},{6,7},{7,6},{8,9},{9,8},{10,11... | collective-permute-start | bytes 491528 | tf_op jit(solution)/shard_map/ppermute | solution.py:39
  3.8 6.3 %collective-permute-start.2 = (s32[10,1,16]{2,1,0:T(1,128)S(1)}, s32[10,1,16]{2,1,0:T(1,128)S(1)}, u32[]{:S(2)}, u32[]{:S(2)}) collective-permute-start(s32[10,1,16]{2,1,0:T(1,128)S(1)} %bitcast.7), channel_id=1, source_target_pairs={{0,6},{2,4},{4,2},{6,0},{1,7},{3,5},{5,3},{7,1},{8,14},{10,12},{12... | collective-permute-start | bytes 1928 | tf_op jit(solution)/shard_map/ppermute | solution.py:25
  8.5 3.6 %collective-permute-start.1 = (s32[10,1,16]{2,1,0:T(1,128)S(1)}, s32[10,1,16]{2,1,0:T(1,128)S(1)}, u32[]{:S(2)}, u32[]{:S(2)}) collective-permute-start(s32[10,1,16]{2,1,0:T(1,128)S(1)} %bitcast.8), channel_id=1, source_target_pairs={{0,2},{1,5},{2,0},{3,7},{4,6},{5,1},{6,4},{7,3},{8,10},{9,13},{10,... | collective-permute-start | bytes 1928 | tf_op jit(solution)/shard_map/ppermute | solution.py:35
  12.5 4.2 %collective-permute-start.3 = (bf16[64,256]{1,0:T(8,128)(2,1)S(1)}, bf16[64,256]{1,0:T(8,128)(2,1)S(1)}, u32[]{:S(2)}, u32[]{:S(2)}) collective-permute-start(bf16[64,256]{1,0:T(8,128)(2,1)S(1)} %get-tuple-element.12), channel_id=1, source_target_pairs={{0,2},{1,5},{2,0},{3,7},{4,6},{5,1},{6,4},{7,3},{8,10},{9,13},{10,... | collective-permute-start | bytes 98312 | tf_op jit(solution)/shard_map/ppermute | solution.py:35
  12.6 6.0 %collective-permute-start.4 = (bf16[32,256]{1,0:T(8,128)(2,1)S(1)}, bf16[32,256]{1,0:T(8,128)(2,1)S(1)}, u32[]{:S(2)}, u32[]{:S(2)}) collective-permute-start(bf16[32,256]{1,0:T(8,128)(2,1)S(1)} %get-tuple-element.13), channel_id=1, source_target_pairs={{0,6},{2,4},{4,2},{6,0},{1,7},{3,5},{5,3},{7,1},{8,14},{10,12},{12... | collective-permute-start | bytes 49160 | tf_op jit(solution)/shard_map/ppermute | solution.py:25
  16.6 2.0 %collective-permute-start.5 = (bf16[32,256]{1,0:T(8,128)(2,1)S(1)}, bf16[32,256]{1,0:T(8,128)(2,1)S(1)}, u32[]{:S(2)}, u32[]{:S(2)}) collective-permute-start(bf16[32,256]{1,0:T(8,128)(2,1)S(1)} %slice.4), channel_id=1, source_target_pairs={{0,1},{1,0},{2,3},{3,2},{4,5},{5,4},{6,7},{7,6},{8,9},{9,8},{10,11... | collective-permute-start | bytes 49160 | tf_op jit(solution)/shard_map/ppermute | solution.py:39
  17.2 3.1 %copy-start.1 = (bf16[512,1024]{1,0:T(8,128)(2,1)S(1)}, bf16[512,1024]{1,0:T(8,128)(2,1)}, u32[]{:S(2)}) copy-start(bf16[512,1024]{1,0:T(8,128)(2,1)} %w_ref.3) | copy-start | bytes 3145732
  19.8 1.5 %collective-permute-start.6 = (bf16[320,256]{1,0:T(8,128)(2,1)S(1)}, bf16[320,256]{1,0:T(8,128)(2,1)S(1)}, u32[]{:S(2)}, u32[]{:S(2)}) collective-permute-start(bf16[320,256]{1,0:T(8,128)(2,1)S(1)} %get-tuple-element.14.own_ref), channel_id=1, source_target_pairs={{0,1},{1,0},{2,3},{3,2},{4,5},{5,4},{6,7},{7,6},{8,9},{9,8},{10,11... | collective-permute-start | bytes 491528 | tf_op jit(solution)/shard_map/ppermute | solution.py:39
